TPU v7x, 32 devices: a whole 2x2x4 slice. The times are simulated.
32 devices in a mesh: rep: 2 (over y), fs: 4 (over z), tp: 4 (over x, core).
Axes of the slice: x: 2, y: 2, z: 4, core: 2. Of those that a mesh axis runs over, the one named last changes fastest.
Arguments:
- stream: bfloat16 [2048, 1536], P(('rep', 'fs')), may hold values from -6 to 6
- mix_pre_gain: float32 [1536], replicated, may hold values from 0.1 to 1.9
- w_outer_gate: bfloat16 [1536, 768], P('fs', 'tp'), may hold values from -0.15625 to 0.15625
- w_inner_gate: bfloat16 [1536, 768], P('fs', 'tp'), may hold values from -0.15625 to 0.15625
- w_value: bfloat16 [1536, 768], P('fs', 'tp'), may hold values from -0.15625 to 0.15625
- mix_taps: float32 [3, 768], P(None, 'tp'), may hold values from -3 to 3
- w_mix_out: bfloat16 [768, 1536], P('tp', 'fs'), may hold values from -0.3125 to 0.3125
- mix_post_gain: float32 [1536], replicated, may hold values from 0.1 to 1.9
- ffn_pre_gain: float32 [1536], replicated, may hold values from 0.1 to 1.9
- w_linear: bfloat16 [1536, 4224], P('fs', 'tp'), may hold values from -0.15625 to 0.15625
- w_gated: bfloat16 [1536, 4224], P('fs', 'tp'), may hold values from -0.15625 to 0.15625
- ffn_taps: float32 [3, 4224], P(None, 'tp'), may hold values from -3 to 3
- ffn_bias: float32 [4224], P('tp'), may hold values from -3 to 3
- w_down: bfloat16 [4224, 1536], P('tp', 'fs'), may hold values from -0.125 to 0.125
- ffn_post_gain: float32 [1536], replicated, may hold values from 0.1 to 1.9
Outputs:
- result: bfloat16 [2048, 1536], P(('rep', 'fs'))
All inputs are finite; a program needn't handle non-finite values.
Results may differ from a plain program's by a relative error of at most 0.023.
Values may be sent and summed in bfloat16 or wider, within the bound.
A program may use at most 64 MiB of HBM per device.

v0:
```python
import functools

import jax
import jax.numpy as jnp
from jax import lax
from jax.experimental import pallas as pl
from jax.experimental.pallas import tpu as pltpu
from jax.sharding import PartitionSpec as P

SEQ_LEN = 128
PACK = 16
CHUNKS = 2


EPS = 1e-06


def norm_scale(values, gain):
    return values * lax.rsqrt(jnp.mean(values * values, axis=-1, keepdims=True) + EPS) * gain


def conv_three(values, taps):
    height, breadth = values.shape
    grouped = values.reshape(height // SEQ_LEN, SEQ_LEN, breadth)
    padded = jnp.pad(grouped, ((0, 0), (1, 1), (0, 0)))
    mixed = taps[0] * padded[:, :-2] + taps[1] * padded[:, 1:-1] + taps[2] * padded[:, 2:]
    return mixed.reshape(height, breadth)


def settle(partial_value, resid, post_gain):
    branch = lax.psum(partial_value.astype(jnp.bfloat16), "tp")
    return (resid + norm_scale(branch.astype(jnp.float32), post_gain)).astype(jnp.bfloat16)


def gather_plan(
    stream,
    mix_pre_gain,
    w_outer_gate,
    w_inner_gate,
    w_value,
    mix_taps,
    w_mix_out,
    mix_post_gain,
    ffn_pre_gain,
    w_linear,
    w_gated,
    ffn_taps,
    ffn_bias,
    w_down,
    ffn_post_gain,
):
    resid = stream.astype(jnp.float32)
    normed = norm_scale(resid, mix_pre_gain).astype(jnp.bfloat16)
    full_outer, full_inner, full_value = (
        lax.all_gather(w_outer_gate, "fs", axis=0, tiled=True),
        lax.all_gather(w_inner_gate, "fs", axis=0, tiled=True),
        lax.all_gather(w_value, "fs", axis=0, tiled=True),
    )
    outer = jnp.dot(normed, full_outer, preferred_element_type=jnp.float32)
    inner = jnp.dot(normed, full_inner, preferred_element_type=jnp.float32)
    value = jnp.dot(normed, full_value, preferred_element_type=jnp.float32)
    outer = outer.astype(jnp.bfloat16)
    inner = inner.astype(jnp.bfloat16)
    value = value.astype(jnp.bfloat16)
    product = inner.astype(jnp.float32) * value.astype(jnp.float32)
    mixed = (outer.astype(jnp.float32) * conv_three(product, mix_taps)).astype(jnp.bfloat16)
    full_mix_out = lax.all_gather(w_mix_out, "fs", axis=1, tiled=True)
    partial_value = jnp.dot(mixed, full_mix_out, preferred_element_type=jnp.float32)
    middle = settle(partial_value, resid, mix_post_gain)
    middle_f = middle.astype(jnp.float32)
    normed_two = norm_scale(middle_f, ffn_pre_gain).astype(jnp.bfloat16)
    full_linear, full_gated = (
        lax.all_gather(w_linear, "fs", axis=0, tiled=True),
        lax.all_gather(w_gated, "fs", axis=0, tiled=True),
    )
    linear = jnp.dot(normed_two, full_linear, preferred_element_type=jnp.float32)
    gated = jnp.dot(normed_two, full_gated, preferred_element_type=jnp.float32)
    linear = linear.astype(jnp.bfloat16)
    gated = gated.astype(jnp.bfloat16)
    activated = jax.nn.gelu(
        conv_three(gated.astype(jnp.float32), ffn_taps) + ffn_bias, approximate=True
    )
    hidden = (activated * linear.astype(jnp.float32)).astype(jnp.bfloat16)
    full_down = lax.all_gather(w_down, "fs", axis=1, tiled=True)
    partial_two = jnp.dot(hidden, full_down, preferred_element_type=jnp.float32)
    return settle(partial_two, middle_f, ffn_post_gain)


ORDER = (1, 3, 2)


def dot_nt(left, right):
    return lax.dot_general(left, right, (((1,), (1,)), ((), ())), preferred_element_type=jnp.float32)


def dot_nn(left, right):
    return jnp.dot(left, right, preferred_element_type=jnp.float32)


def conv_rows(values, taps):
    height = values.shape[0]
    row = lax.broadcasted_iota(jnp.int32, values.shape, 0) % SEQ_LEN
    before = jnp.where(row == 0, 0.0, pltpu.roll(values, 1, 0))
    after = jnp.where(row == SEQ_LEN - 1, 0.0, pltpu.roll(values, height - 1, 0))
    return taps[0:1] * before + taps[1:2] * values + taps[2:3] * after


def kernel(
    n_fs,
    conv_w,
    hid,
    stream,
    gain_mix_pre,
    gain_mix_post,
    gain_ffn_pre,
    gain_ffn_post,
    w_outer,
    w_inner,
    w_value,
    w_mix_out,
    mix_taps,
    w_linear,
    w_gated,
    w_down,
    ffn_taps,
    ffn_bias,
    out,
    small_all,
    ffn_w,
    mix_all,
    ffn_all,
    xs,
    normed,
    middle,
    pm,
    rm,
    sm,
    rxm,
    bm,
    pf,
    rf,
    sf,
    rxf,
    tf,
    rz,
    bf,
    zs_s,
    zs_r,
    mix_s,
    mix_r,
    ag_s,
    ag_r,
    rs_s,
    rs_r,
    fin_s,
    fin_r,
):
    r, f, t = lax.axis_index("rep"), lax.axis_index("fs"), lax.axis_index("tp")
    x, c = t // 2, t % 2
    core = {"tp": 2 * x + 1 - c}
    side = {"tp": 2 * (1 - x) + c}
    t_side = 2 * (1 - x) + c
    other = {"rep": 1 - r}
    rows, width = stream.shape[0], w_value.shape[1]
    units = w_linear.shape[1]
    n_seq = rows // SEQ_LEN
    mix_half, ffn_half = mix_all.shape[1] // 2, ffn_w.shape[1] // 2

    def send(src, dst, ss, rs, where):
        return pltpu.make_async_remote_copy(
            src_ref=src,
            dst_ref=dst,
            send_sem=ss,
            recv_sem=rs,
            device_id=where,
            device_id_type=pl.DeviceIdType.MESH,
        )

    barrier = pltpu.get_barrier_semaphore()
    peers = [core, side, other] + [{"fs": (f + k) % n_fs} for k in ORDER]
    for peer in peers:
        pl.semaphore_signal(barrier, inc=1, device_id=peer, device_id_type=pl.DeviceIdType.MESH)
    for p, piece in enumerate((w_outer, w_inner, w_value, w_mix_out)):
        mix_all[f, p * conv_w : (p + 1) * conv_w] = piece[...]
    pl.semaphore_wait(barrier, len(peers))

    mix_cut, ffn_cut = mix_half // CHUNKS, ffn_half // CHUNKS
    mix_rows = [pl.ds(pl.multiple_of(r * mix_half + h * mix_cut, PACK), mix_cut) for h in range(CHUNKS)]
    ffn_rows = [pl.ds(pl.multiple_of(r * ffn_half + h * ffn_cut, PACK), ffn_cut) for h in range(CHUNKS)]
    cuts = [(k, h) for k in ORDER for h in range(CHUNKS)]
    mix_z, ffn_z = {}, {}
    for k, h in cuts:
        to = {"fs": (f + k) % n_fs}
        src = mix_all.at[f, mix_rows[h]]
        mix_z[k, h] = send(src, src, zs_s.at[0, k, h], zs_r.at[0, k, h], to)
        mix_z[k, h].start()
    for p, piece in enumerate((w_linear, w_gated, w_down)):
        end = (p + 1) * hid if p < 2 else ffn_w.shape[1]
        edge = units // PACK * PACK
        for j in range(n_fs):
            ffn_w[j, p * hid + edge : end] = jnp.zeros((end - p * hid - edge, width), ffn_w.dtype)
            ffn_w[j, p * hid : p * hid + units] = piece[j]
    for k, h in cuts:
        to = (f + k) % n_fs
        src, dst = ffn_w.at[to, ffn_rows[h]], ffn_all.at[f, ffn_rows[h]]
        ffn_z[k, h] = send(src, dst, zs_s.at[1, k, h], zs_r.at[1, k, h], {"fs": to})
        ffn_z[k, h].start()

    ffn_all[f] = ffn_w[f]
    small_all[...] = jnp.zeros(small_all.shape, jnp.float32)
    for j in range(n_fs):
        small_all[j, 0:3, 0:units] = ffn_taps[:, j * units : (j + 1) * units]
        small_all[j, 3:4, 0:units] = ffn_bias[j * units : (j + 1) * units][None]

    def norm_rows(values, gain):
        scale = lax.rsqrt(jnp.mean(values * values, axis=-1, keepdims=True) + EPS)
        return values * scale * gain

    step_rows = 32

    @pl.loop(0, rows // step_rows)
    def _(i):
        at = pl.ds(pl.multiple_of(i * step_rows, step_rows), step_rows)
        normed[at] = norm_rows(stream[at].astype(jnp.float32), gain_mix_pre[...][None]).astype(jnp.bfloat16)

    mix_y = {}
    for k, h in cuts:
        mix_z[k, h].wait_recv()
        src = mix_all.at[(f - k + n_fs) % n_fs, mix_rows[h]]
        mix_y[k, h] = send(src, src, zs_s.at[2, k, h], zs_r.at[2, k, h], other)
        mix_y[k, h].start()
    for k, h in cuts:
        mix_y[k, h].wait_recv()

    mix_core, mix_side, mix_back = {}, {}, {}
    for q in range(n_seq):
        here = slice(q * SEQ_LEN, (q + 1) * SEQ_LEN)
        parts = []
        for p in range(3):
            total = 0.0
            for j in range(n_fs):
                total = total + dot_nt(
                    normed[here, j * width : (j + 1) * width], mix_all[j, p * conv_w : (p + 1) * conv_w]
                )
            parts.append(total.astype(jnp.bfloat16).astype(jnp.float32))
        mixed = (parts[0] * conv_rows(parts[1] * parts[2], mix_taps)).astype(jnp.bfloat16)
        for j in range(n_fs):
            pm[q, j % 2, j // 2] = dot_nn(mixed, mix_all[j, 3 * conv_w : 4 * conv_w]).astype(jnp.bfloat16)
        mix_core[q] = send(pm.at[q, 1 - c], rm.at[q], mix_s.at[0, q], mix_r.at[0, q], core)
        mix_core[q].start()
    for q in range(n_seq):
        mix_core[q].wait_recv()
        sm[q] = (pm[q, c].astype(jnp.float32) + rm[q].astype(jnp.float32)).astype(jnp.bfloat16)
        mix_side[q] = send(sm.at[q], rxm.at[q], mix_s.at[1, q], mix_r.at[1, q], side)
        mix_side[q].start()
    ffn_y = {}

    def forward(k):
        for h in range(CHUNKS):
            ffn_z[k, h].wait_recv()
            src = ffn_all.at[(f - k + n_fs) % n_fs, ffn_rows[h]]
            ffn_y[k, h] = send(src, src, zs_s.at[3, k, h], zs_r.at[3, k, h], other)
            ffn_y[k, h].start()

    for q in range(n_seq):
        mix_side[q].wait_recv()
        bm[q, c] = (sm[q].astype(jnp.float32) + rxm[q].astype(jnp.float32)).astype(jnp.bfloat16)
        mix_back[q] = send(bm.at[q, c], bm.at[q, c], mix_s.at[2, q], mix_r.at[2, q], core)
        mix_back[q].start()
    ag_z, ag_side, ag_core, ag_fwd = {}, {}, {}, {}
    forward(ORDER[0])
    forward(ORDER[1])
    for q in range(n_seq):
        mix_back[q].wait_recv()

        @pl.loop(0, SEQ_LEN // step_rows)
        def _(i):
            at = pl.ds(pl.multiple_of(i * step_rows, step_rows), step_rows)
            to = pl.ds(pl.multiple_of(q * SEQ_LEN + i * step_rows, step_rows), step_rows)
            branch = jnp.concatenate([bm[q, j % 2, j // 2, at] for j in range(n_fs)], axis=1)
            mid = stream[to].astype(jnp.float32) + norm_rows(branch.astype(jnp.float32), gain_mix_post[...][None])
            mid = mid.astype(jnp.bfloat16)
            middle[to] = mid
            two = norm_rows(mid.astype(jnp.float32), gain_ffn_pre[...][None]).astype(jnp.bfloat16)
            for j in range(n_fs):
                xs[f, j, to] = two[:, j * width : (j + 1) * width]

        for k in ORDER:
            src = xs.at[f, t, q * SEQ_LEN : (q + 1) * SEQ_LEN]
            ag_z[k, q] = send(src, src, ag_s.at[0, k, q], ag_r.at[0, k, q], {"fs": (f + k) % n_fs})
            ag_z[k, q].start()

    forward(ORDER[2])

    def spread(k, q):
        ag_z[k, q].wait_recv()
        src = xs.at[(f - k + n_fs) % n_fs, t, q * SEQ_LEN : (q + 1) * SEQ_LEN]
        ag_side[k, q] = send(src, src, ag_s.at[1, k, q], ag_r.at[1, k, q], side)
        ag_side[k, q].start()
        ag_core[k, q] = send(src, src, ag_s.at[2, k, q], ag_r.at[2, k, q], core)
        ag_core[k, q].start()

    def pass_on(k, q):
        ag_side[k, q].wait_recv()
        src = xs.at[(f - k + n_fs) % n_fs, t_side, q * SEQ_LEN : (q + 1) * SEQ_LEN]
        ag_fwd[k, q] = send(src, src, ag_s.at[3, k, q], ag_r.at[3, k, q], core)
        ag_fwd[k, q].start()

    rs_core, rs_side, rs_z = {}, {}, {}

    def block(k, q):
        if k > 0:
            ag_core[k, q].wait_recv()
            ag_fwd[k, q].wait_recv()
        z = (f - k + n_fs) % n_fs
        small = small_all[f]
        linear, gated = 0.0, 0.0
        for j in range(n_fs):
            act = xs[z, j, q * SEQ_LEN : (q + 1) * SEQ_LEN]
            linear = linear + dot_nt(act, ffn_all[j, 0:hid])
            gated = gated + dot_nt(act, ffn_all[j, hid : 2 * hid])
        linear = linear.astype(jnp.bfloat16).astype(jnp.float32)
        gated = gated.astype(jnp.bfloat16).astype(jnp.float32)
        act = jax.nn.gelu(conv_rows(gated, small) + small[3:4], approximate=True)
        hidden = (act * linear).astype(jnp.bfloat16)
        for j in range(n_fs):
            pf[k, q, j % 2, j // 2] = dot_nn(hidden, ffn_all[j, 2 * hid : 3 * hid]).astype(jnp.bfloat16)
        rs_core[k, q] = send(pf.at[k, q, 1 - c], rf.at[k, q], rs_s.at[0, k, q], rs_r.at[0, k, q], core)
        rs_core[k, q].start()

    def stage_core(k, q):
        rs_core[k, q].wait_recv()
        theirs = pf[k, q, c, 1 - x].astype(jnp.float32) + rf[k, q, 1 - x].astype(jnp.float32)
        sf[k, q, 1 - x] = theirs.astype(jnp.bfloat16)
        rs_side[k, q] = send(sf.at[k, q, 1 - x], rxf.at[k, q], rs_s.at[1, k, q], rs_r.at[1, k, q], side)
        rs_side[k, q].start()
        ours = pf[k, q, c, x].astype(jnp.float32) + rf[k, q, x].astype(jnp.float32)
        sf[k, q, x] = ours.astype(jnp.bfloat16)

    def stage_side(k, q):
        rs_side[k, q].wait_recv()
        tf[k, q] = (sf[k, q, x].astype(jnp.float32) + rxf[k, q].astype(jnp.float32)).astype(jnp.bfloat16)
        if k > 0:
            to = {"fs": (f - k + n_fs) % n_fs}
            rs_z[k, q] = send(tf.at[k, q], rz.at[k, q], rs_s.at[2, k, q], rs_r.at[2, k, q], to)
            rs_z[k, q].start()

    own = [(0, q) for q in range(n_seq)]
    work = [(k, q) for k in ORDER for q in range(n_seq)]
    lag = len(own)
    every = own + work
    for i in range(len(work) + 6):
        if i < len(work):
            spread(*work[i])
        if i == 0:
            for cut in cuts:
                ffn_y[cut].wait_recv()
        if i < lag:
            block(*own[i])
        if 1 <= i <= len(work):
            pass_on(*work[i - 1])
        if 2 <= i < len(work) + 2:
            block(*work[i - 2])
        if 1 <= i <= len(every):
            stage_core(*every[i - 1])
        if 3 <= i < len(every) + 3:
            stage_side(*every[i - 3])

    fin_side, fin_core, fin_fwd = {}, {}, {}
    for q in range(n_seq):
        at = slice(q * SEQ_LEN, (q + 1) * SEQ_LEN)
        total = tf[0, q].astype(jnp.float32)
        for k in ORDER:
            rs_z[k, q].wait_recv()
            total = total + rz[k, q].astype(jnp.float32)
        bf[t, at] = total.astype(jnp.bfloat16)
        mine = bf.at[t, at]
        fin_side[q] = send(mine, mine, fin_s.at[0, q], fin_r.at[0, q], side)
        fin_side[q].start()
        fin_core[q] = send(mine, mine, fin_s.at[1, q], fin_r.at[1, q], core)
        fin_core[q].start()
    for q in range(n_seq):
        fin_side[q].wait_recv()
        theirs = bf.at[t_side, q * SEQ_LEN : (q + 1) * SEQ_LEN]
        fin_fwd[q] = send(theirs, theirs, fin_s.at[2, q], fin_r.at[2, q], core)
        fin_fwd[q].start()
    for q in range(n_seq):
        fin_core[q].wait_recv()
        fin_fwd[q].wait_recv()

    @pl.loop(0, rows // step_rows)
    def _(i):
        at = pl.ds(pl.multiple_of(i * step_rows, step_rows), step_rows)
        branch = jnp.concatenate([bf[j, at] for j in range(n_fs)], axis=1).astype(jnp.float32)
        out[at] = (middle[at].astype(jnp.float32) + norm_rows(branch, gain_ffn_post[...][None])).astype(jnp.bfloat16)

    groups = [mix_z, ffn_z, mix_y, ffn_y, mix_core, mix_side, mix_back]
    groups += [ag_z, ag_side, ag_core, ag_fwd, rs_core, rs_side, rs_z]
    groups += [fin_side, fin_core, fin_fwd]
    for group in groups:
        for copy in group.values():
            copy.wait_send()


def split_plan(
    n_fs,
    stream,
    mix_pre_gain,
    w_outer_gate,
    w_inner_gate,
    w_value,
    mix_taps,
    w_mix_out,
    mix_post_gain,
    ffn_pre_gain,
    w_linear,
    w_gated,
    ffn_taps,
    ffn_bias,
    w_down,
    ffn_post_gain,
):
    rows, model = stream.shape
    width, conv_w = w_value.shape
    units = w_linear.shape[1] // n_fs
    hid = -(-units // PACK) * PACK
    deep = -(-3 * hid // (2 * CHUNKS * PACK)) * 2 * CHUNKS * PACK
    cut = lambda rows_of: rows_of.reshape(n_fs, units, width)
    n_seq = rows // SEQ_LEN
    half = jnp.bfloat16
    vmem, dma = pltpu.VMEM, pltpu.SemaphoreType.DMA
    return pl.pallas_call(
        functools.partial(kernel, n_fs, conv_w, hid),
        out_shape=jax.ShapeDtypeStruct((rows, model), half),
        in_specs=[pl.BlockSpec(memory_space=vmem)] * 15,
        out_specs=pl.BlockSpec(memory_space=vmem),
        scratch_shapes=[
            vmem((n_fs, 8, hid), jnp.float32),
            vmem((n_fs, deep, width), half),
            vmem((n_fs, 4 * conv_w, width), half),
            vmem((n_fs, deep, width), half),
            vmem((n_fs, n_fs, rows, width), half),
            vmem((rows, model), half),
            vmem((rows, model), half),
            vmem((n_seq, 2, 2, SEQ_LEN, width), half),
            vmem((n_seq, 2, SEQ_LEN, width), half),
            vmem((n_seq, 2, SEQ_LEN, width), half),
            vmem((n_seq, 2, SEQ_LEN, width), half),
            vmem((n_seq, 2, 2, SEQ_LEN, width), half),
            vmem((n_fs, n_seq, 2, 2, SEQ_LEN, width), half),
            vmem((n_fs, n_seq, 2, SEQ_LEN, width), half),
            vmem((n_fs, n_seq, 2, SEQ_LEN, width), half),
            vmem((n_fs, n_seq, SEQ_LEN, width), half),
            vmem((n_fs, n_seq, SEQ_LEN, width), half),
            vmem((n_fs, n_seq, SEQ_LEN, width), half),
            vmem((n_fs, rows, width), half),
            dma((4, n_fs, CHUNKS)),
            dma((4, n_fs, CHUNKS)),
            dma((3, n_seq)),
            dma((3, n_seq)),
            dma((4, n_fs, n_seq)),
            dma((4, n_fs, n_seq)),
            dma((3, n_fs, n_seq)),
            dma((3, n_fs, n_seq)),
            dma((3, n_seq)),
            dma((3, n_seq)),
        ],
        compiler_params=pltpu.CompilerParams(
            collective_id=0, has_side_effects=True, vmem_limit_bytes=56 * 2**20
        ),
    )(
        stream,
        mix_pre_gain,
        mix_post_gain,
        ffn_pre_gain,
        ffn_post_gain,
        w_outer_gate.T,
        w_inner_gate.T,
        w_value.T,
        w_mix_out,
        mix_taps,
        cut(w_linear.T),
        cut(w_gated.T),
        cut(w_down),
        ffn_taps,
        ffn_bias,
    )


def on_device(rep, n_fs, n_tp, *arrays):
    stream, w_value, w_linear = arrays[0], arrays[4], arrays[9]
    same = n_fs == n_tp == 2 * rep == len(ORDER) + 1
    whole = w_value.shape[0] % 128 == 0 and w_value.shape[1] % (CHUNKS * PACK) == 0
    even = w_linear.shape[1] % n_fs == 0 and stream.shape[0] % SEQ_LEN == 0
    if same and rep == 2 and whole and even:
        return split_plan(n_fs, *arrays)
    return gather_plan(*arrays)


def solution(mesh):
    in_specs = (
        P(("rep", "fs"), None),
        P(),
        P("fs", "tp"),
        P("fs", "tp"),
        P("fs", "tp"),
        P(None, "tp"),
        P("tp", "fs"),
        P(),
        P(),
        P("fs", "tp"),
        P("fs", "tp"),
        P(None, "tp"),
        P("tp"),
        P("tp", "fs"),
        P(),
    )
    out_specs = P(("rep", "fs"), None)
    sizes = mesh.shape
    body = functools.partial(on_device, sizes["rep"], sizes["fs"], sizes["tp"])
    return jax.shard_map(
        body, mesh=mesh, in_specs=in_specs, out_specs=out_specs, check_vma=False
    )
```

profile of v0, /device:TPU:0, one launch (start us, length us, event | category | flops | bytes accessed | tf_op | source)
XLA Modules:
  0.0 126.5 jit_solution(3657019522133308963)
XLA Ops:
  0.0 124.4 %shard_map.145 = bf16[256,1536]{1,0:T(8,128)(2,1)} custom-call(bf16[256,1536]{1,0:T(8,128)(2,1)} %stream.1, f32[1536]{0:T(1024)} %gain_mix_pre.1, f32[1536]{0:T(1024)} %gain_mix_post.1, f32[1536]{0:T(1024)} %gain_ffn_pre.1, f32[1536]{0:T(1024)} %gain_ffn_post.1, bf16[192,384]{1,0:T(8,128)(2,1)} %bitcast.13, bf16[192,384]{1,0:T(8,128)(2,1)} %bitcast.14, ...), custom_call_target="tpu_custom_call" | custom-call | tf_op jit(solution)/shard_map/pallas_call | solution.py:432
  124.4 2.1 %copy.17 = bf16[256,1536]{1,0:T(8,128)(2,1)} copy(bf16[256,1536]{1,0:T(8,128)(2,1)} %shard_map.145) | data formatting | bytes 1572864
where the time goes:
time: 127 us; the launch traced here: 126 us
  Pallas kernels  124 us (98%)
  local copies, waits for them, and re-layouts  2.06 us (2%)
    pallas_call x1, Pallas kernels, split_plan(): pl.pallas_call(functools.partial(kernel, n_fs, conv_w, hid), out_shape=ja...  124 us

commit v1 on v0

v1 whole, which is shorter than its diff:
```python
import contextlib
import functools

import jax
import jax.numpy as jnp
from jax import lax
from jax.experimental import pallas as pl
from jax.experimental.pallas import tpu as pltpu
from jax.sharding import PartitionSpec as P

SEQ_LEN = 128
PACK = 16
CHUNKS = 2
SPREAD = 2
TRACE = False


EPS = 1e-06


def norm_scale(values, gain):
    return values * lax.rsqrt(jnp.mean(values * values, axis=-1, keepdims=True) + EPS) * gain


def conv_three(values, taps):
    height, breadth = values.shape
    grouped = values.reshape(height // SEQ_LEN, SEQ_LEN, breadth)
    padded = jnp.pad(grouped, ((0, 0), (1, 1), (0, 0)))
    mixed = taps[0] * padded[:, :-2] + taps[1] * padded[:, 1:-1] + taps[2] * padded[:, 2:]
    return mixed.reshape(height, breadth)


def settle(partial_value, resid, post_gain):
    branch = lax.psum(partial_value.astype(jnp.bfloat16), "tp")
    return (resid + norm_scale(branch.astype(jnp.float32), post_gain)).astype(jnp.bfloat16)


def gather_plan(
    stream,
    mix_pre_gain,
    w_outer_gate,
    w_inner_gate,
    w_value,
    mix_taps,
    w_mix_out,
    mix_post_gain,
    ffn_pre_gain,
    w_linear,
    w_gated,
    ffn_taps,
    ffn_bias,
    w_down,
    ffn_post_gain,
):
    resid = stream.astype(jnp.float32)
    normed = norm_scale(resid, mix_pre_gain).astype(jnp.bfloat16)
    full_outer, full_inner, full_value = (
        lax.all_gather(w_outer_gate, "fs", axis=0, tiled=True),
        lax.all_gather(w_inner_gate, "fs", axis=0, tiled=True),
        lax.all_gather(w_value, "fs", axis=0, tiled=True),
    )
    outer = jnp.dot(normed, full_outer, preferred_element_type=jnp.float32)
    inner = jnp.dot(normed, full_inner, preferred_element_type=jnp.float32)
    value = jnp.dot(normed, full_value, preferred_element_type=jnp.float32)
    outer = outer.astype(jnp.bfloat16)
    inner = inner.astype(jnp.bfloat16)
    value = value.astype(jnp.bfloat16)
    product = inner.astype(jnp.float32) * value.astype(jnp.float32)
    mixed = (outer.astype(jnp.float32) * conv_three(product, mix_taps)).astype(jnp.bfloat16)
    full_mix_out = lax.all_gather(w_mix_out, "fs", axis=1, tiled=True)
    partial_value = jnp.dot(mixed, full_mix_out, preferred_element_type=jnp.float32)
    middle = settle(partial_value, resid, mix_post_gain)
    middle_f = middle.astype(jnp.float32)
    normed_two = norm_scale(middle_f, ffn_pre_gain).astype(jnp.bfloat16)
    full_linear, full_gated = (
        lax.all_gather(w_linear, "fs", axis=0, tiled=True),
        lax.all_gather(w_gated, "fs", axis=0, tiled=True),
    )
    linear = jnp.dot(normed_two, full_linear, preferred_element_type=jnp.float32)
    gated = jnp.dot(normed_two, full_gated, preferred_element_type=jnp.float32)
    linear = linear.astype(jnp.bfloat16)
    gated = gated.astype(jnp.bfloat16)
    activated = jax.nn.gelu(
        conv_three(gated.astype(jnp.float32), ffn_taps) + ffn_bias, approximate=True
    )
    hidden = (activated * linear.astype(jnp.float32)).astype(jnp.bfloat16)
    full_down = lax.all_gather(w_down, "fs", axis=1, tiled=True)
    partial_two = jnp.dot(hidden, full_down, preferred_element_type=jnp.float32)
    return settle(partial_two, middle_f, ffn_post_gain)


def dot_nt(left, right):
    return lax.dot_general(left, right, (((1,), (1,)), ((), ())), preferred_element_type=jnp.float32)


def dot_nn(left, right):
    return jnp.dot(left, right, preferred_element_type=jnp.float32)


def conv_rows(values, taps):
    height = values.shape[0]
    row = lax.broadcasted_iota(jnp.int32, values.shape, 0) % SEQ_LEN
    before = jnp.where(row == 0, 0.0, pltpu.roll(values, 1, 0))
    after = jnp.where(row == SEQ_LEN - 1, 0.0, pltpu.roll(values, height - 1, 0))
    return taps[0:1] * before + taps[1:2] * values + taps[2:3] * after


def norm_rows(values, gain):
    scale = lax.rsqrt(jnp.mean(values * values, axis=-1, keepdims=True) + EPS)
    return values * scale * gain


def scope(name):
    return jax.named_scope(name) if TRACE else contextlib.nullcontext()


def kernel(
    n_fs,
    conv_w,
    low,
    cap,
    stream,
    gain_mix_pre,
    gain_mix_post,
    gain_ffn_pre,
    gain_ffn_post,
    w_outer,
    w_inner,
    w_value,
    w_mix_out,
    mix_taps,
    w_linear,
    w_gated,
    w_down,
    ffn_taps,
    ffn_bias,
    out,
    small_all,
    smalls,
    ffn_w,
    ffn_all,
    mix_all,
    normed,
    pm,
    rm,
    sm,
    rxm,
    middle,
    xs,
    pf,
    rf,
    sf,
    rx,
    tf,
    rz,
    mz_s,
    mz_r,
    my_s,
    my_r,
    mr_s,
    mr_r,
    fz_s,
    fz_r,
    fy_s,
    fy_r,
    fx_s,
    fx_r,
    az_s,
    az_r,
    ap_s,
    ap_r,
    rs_s,
    rs_r,
    rz_s,
    rz_r,
    fin_s,
    fin_r,
):
    r, f, t = lax.axis_index("rep"), lax.axis_index("fs"), lax.axis_index("tp")
    x, c = t // 2, t % 2
    t_core, t_side = 2 * x + 1 - c, 2 * (1 - x) + c
    core, side, other = {"tp": t_core}, {"tp": t_side}, {"rep": 1 - r}
    rows, width = stream.shape[0], w_value.shape[1]
    units = w_linear.shape[1]
    share = rows // 4
    mine = pl.ds(pl.multiple_of(c * share, share), share)
    theirs = pl.ds(pl.multiple_of((1 - c) * share, share), share)
    high = units - low

    near = f < n_fs // 2
    mirror = lambda v: jnp.where(near, v, n_fs - 1 - v)
    inner = jnp.where(near, f, n_fs - 1 - f) == 1
    edge = jnp.logical_not(inner)
    order = [mirror(jnp.where(inner, 0, 1)), mirror(2), mirror(3)]
    goals = [mirror(jnp.where(inner, 2, 1)), mirror(jnp.where(inner, 3, 2)), mirror(jnp.where(inner, 0, 3))]
    upward, downward = mirror(jnp.where(inner, 2, 1)), mirror(0)
    places = [f] + order

    started = []

    def send(src, dst, ss, rs, where):
        return pltpu.make_async_remote_copy(
            src_ref=src,
            dst_ref=dst,
            send_sem=ss,
            recv_sem=rs,
            device_id=where,
            device_id_type=pl.DeviceIdType.MESH,
        )

    def start(copy, when=None):
        started.append((copy, when))
        if when is None:
            copy.start()
        else:
            pl.when(when)(copy.start)

    def wait(copy, name):
        with scope(name):
            copy.wait_recv()

    barrier = pltpu.get_barrier_semaphore()
    peers = [core, side, other] + [{"fs": (f + k) % n_fs} for k in (1, 2, 3)]
    for peer in peers:
        pl.semaphore_signal(barrier, inc=1, device_id=peer, device_id_type=pl.DeviceIdType.MESH)
    for p, piece in enumerate((w_outer, w_inner, w_value, w_mix_out)):
        mix_all[f, p * conv_w : (p + 1) * conv_w] = piece[...]
    with scope("barrier"):
        pl.semaphore_wait(barrier, len(peers))

    mix_half = mix_all.shape[1] // 2
    mix_cut = mix_half // CHUNKS

    def mix_copy(b, h, slot, to):
        at = pl.ds(pl.multiple_of(r * mix_half + h * mix_cut, PACK), mix_cut)
        ref = mix_all.at[b, at]
        return send(ref, ref, mz_s.at[slot], mz_r.at[b, h], {"fs": to})

    for h in range(CHUNKS):
        start(mix_copy(f, h, h, upward))
        start(mix_copy(f, h, CHUNKS + h, downward), inner)

    for p, piece in enumerate((w_linear, w_gated, w_down)):
        for j in range(n_fs):
            ffn_w[j, p, low:cap] = jnp.zeros((cap - low, width), ffn_w.dtype)

        @pl.when(r == 0)
        def _():
            for j in range(n_fs):
                ffn_w[j, p, 0:low] = piece[j, 0:low]

        @pl.when(r == 1)
        def _():
            for j in range(n_fs):
                ffn_w[j, p, 0:high] = piece[j, low:units]

    def ffn_send(i):
        for p in range(3):
            src, dst = ffn_w.at[goals[i], p], ffn_all.at[f, 0, p]
            yield send(src, dst, fz_s.at[i, p], fz_r.at[f, p], {"fs": goals[i]})

    ffn_out = [list(ffn_send(i)) for i in range(3)]
    started += [(copy, None) for copies in ffn_out for copy in copies]

    def ffn_start(*which):
        for i in which:
            for copy in ffn_out[i]:
                copy.start()

    pl.when(edge)(functools.partial(ffn_start, 0, 1, 2))

    def ffn_side(i):
        for p in range(3):
            src = ffn_w.at[f, p] if i == 0 else ffn_all.at[places[i], 0, p]
            dst = ffn_all.at[places[i], 2, p]
            yield send(src, dst, fx_s.at[i, p], fx_r.at[i, p], side)

    fx = [list(ffn_side(i)) for i in range(4)]
    for copy in fx[0]:
        start(copy)
    for p, piece in enumerate((w_linear, w_gated, w_down)):
        ffn_all[f, 0, p] = ffn_w[f, p]
        ffn_all[f, 1, p, low:cap] = jnp.zeros((cap - low, width), ffn_w.dtype)

        @pl.when(r == 0)
        def _():
            ffn_all[f, 1, p, 0:high] = piece[f, low:units]

        @pl.when(r == 1)
        def _():
            ffn_all[f, 1, p, 0:low] = piece[f, 0:low]

    small_all[...] = jnp.zeros(small_all.shape, jnp.float32)
    for j in range(n_fs):
        for half, size in enumerate((low, high)):
            at = j * units + half * low
            small_all[j, half, 0:3, 0:size] = ffn_taps[:, at : at + size]
            small_all[j, half, 3:4, 0:size] = ffn_bias[at : at + size][None]
    smalls[0] = small_all[f, r]
    smalls[1] = small_all[f, 1 - r]
    small_copy = send(smalls.at[0], smalls.at[2], fx_s.at[4, 0], fx_r.at[4, 0], side)
    start(small_copy)

    step_rows = 32

    @pl.loop(0, rows // step_rows)
    def _(i):
        at = pl.ds(pl.multiple_of(i * step_rows, step_rows), step_rows)
        normed[at] = norm_rows(stream[at].astype(jnp.float32), gain_mix_pre[...][None]).astype(jnp.bfloat16)

    flows = [(i, h) for i in range(3) for h in range(CHUNKS)]
    turns = [(i, h) for h in range(CHUNKS) for i in range(2)] + [(2, h) for h in range(CHUNKS)]
    my = []
    for e in range(3 * CHUNKS):
        (i_edge, h_edge), (i_inner, h_inner) = flows[e], turns[e]
        b = jnp.where(inner, order[i_inner], order[i_edge])
        h = jnp.where(inner, h_inner, h_edge)
        onward = downward if i_inner > 0 else upward
        copy = mix_copy(b, h, 2 * CHUNKS + e, onward)
        wait(copy, f"mixz_{e}")
        start(copy, inner)
        at = pl.ds(pl.multiple_of(r * mix_half + h * mix_cut, PACK), mix_cut)
        ref = mix_all.at[b, at]
        my.append(send(ref, ref, my_s.at[e], my_r.at[e], other))
        start(my[e])
        if e == 2 * CHUNKS - 2:
            pl.when(inner)(functools.partial(ffn_start, 0, 1))
    pl.when(inner)(functools.partial(ffn_start, 2))

    fy = []
    for i in range(1, 4):
        fy.append([])
        for p in range(3):
            src, dst = ffn_all.at[places[i], 0, p], ffn_all.at[places[i], 1, p]
            fy[-1].append(send(src, dst, fy_s.at[i - 1, p], fy_r.at[i - 1, p], other))

    def forward(i):
        for p in range(3):
            src = ffn_all.at[places[i], 0, p]
            wait(send(src, src, fz_s.at[i - 1, p], fz_r.at[places[i], p], other), f"ffnz_{i}_{p}")
            fy[i - 1][p].start()
            fx[i][p].start()

    for i in range(1, 4):
        started.extend((copy, None) for copy in fy[i - 1])
        started.extend((copy, None) for copy in fx[i])

    @pl.when(inner)
    def _():
        forward(1)

    for e in range(3 * CHUNKS):
        wait(my[e], f"mixy_{e}")

    mix_core = []
    for k, q in enumerate((1 - x, x)):
        here = pl.ds(pl.multiple_of(q * SEQ_LEN, SEQ_LEN), SEQ_LEN)
        parts = []
        for p in range(3):
            total = 0.0
            for j in range(n_fs):
                total = total + dot_nt(
                    normed[here, j * width : (j + 1) * width], mix_all[j, p * conv_w : (p + 1) * conv_w]
                )
            parts.append(total.astype(jnp.bfloat16).astype(jnp.float32))
        mixed = (parts[0] * conv_rows(parts[1] * parts[2], mix_taps)).astype(jnp.bfloat16)
        for j in range(n_fs):
            pm[k, :, j * width : (j + 1) * width] = dot_nn(
                mixed, mix_all[j, 3 * conv_w : 4 * conv_w]
            ).astype(jnp.bfloat16)
        mix_core.append(send(pm.at[k, theirs], rm.at[k], mr_s.at[k], mr_r.at[k], core))
        start(mix_core[k])

    def mix_sum(k):
        wait(mix_core[k], f"mixcore_{k}")
        return (pm[k, mine].astype(jnp.float32) + rm[k].astype(jnp.float32)).astype(jnp.bfloat16)

    sm[...] = mix_sum(0)
    mix_side = send(sm, rxm, mr_s.at[2], mr_r.at[2], side)
    start(mix_side)

    @pl.when(edge)
    def _():
        forward(1)

    kept = mix_sum(1)
    forward(2)
    wait(mix_side, "mixside")
    branch = (kept.astype(jnp.float32) + rxm[...].astype(jnp.float32)).astype(jnp.bfloat16)
    slot = pl.ds(pl.multiple_of(t * share, share), share)
    mid = stream[slot].astype(jnp.float32) + norm_rows(branch.astype(jnp.float32), gain_mix_post[...][None])
    mid = mid.astype(jnp.bfloat16)
    middle[...] = mid
    xs[f, 0, mine] = norm_rows(mid.astype(jnp.float32), gain_ffn_pre[...][None]).astype(jnp.bfloat16)

    across = [z % 2 == 0 for z in places]
    partner = [{"rep": jnp.where(a, r, 1 - r), "tp": jnp.where(a, t_side, t)} for a in across]
    cut = share // SPREAD

    def piece_of(z, s, a):
        return xs.at[z, s, pl.ds(pl.multiple_of(c * share + a * cut, cut), cut)]

    ag_core, ag_pair, ag_pass = {}, {}, {}

    def spread(i):
        z = places[i]
        for a in range(SPREAD):
            src = piece_of(z, 0, a)
            if i == 0:
                start(send(src, src, az_s.at[0, a], az_r.at[z, a], {"fs": upward}))
                start(send(src, src, az_s.at[1, a], az_r.at[z, a], {"fs": downward}), inner)
            else:
                onward = downward if i > 1 else upward
                copy = send(src, src, az_s.at[1 + i, a], az_r.at[z, a], {"fs": onward})
                wait(copy, f"agz_{i}_{a}")
                start(copy, inner)
            ag_pair[i, a] = send(src, piece_of(z, 1, a), ap_s.at[0, i, a], ap_r.at[0, i, a], partner[i])
            start(ag_pair[i, a])
            ag_core[i, a] = send(src, src, ap_s.at[1, i, a], ap_r.at[1, i, a], core)
            start(ag_core[i, a])

    def pass_on(i):
        for a in range(SPREAD):
            wait(ag_pair[i, a], f"agpair_{i}_{a}")
            src = piece_of(places[i], 1, a)
            ag_pass[i, a] = send(src, src, ap_s.at[2, i, a], ap_r.at[2, i, a], core)
            start(ag_pass[i, a])

    rs_core, rs_pair, rs_z = {}, {}, {}

    def block(i, s):
        for a in range(SPREAD):
            wait((ag_pass if s else ag_core)[i, a], f"agcore_{i}_{s}_{a}")
        z = places[i]
        second = jnp.where(across[i], 1, 2)
        hidden = []
        for h in (0, second):
            linear, gated = 0.0, 0.0
            for j in range(n_fs):
                act = xs[z, s, :, j * width : (j + 1) * width]
                linear = linear + dot_nt(act, ffn_all[j, h, 0])
                gated = gated + dot_nt(act, ffn_all[j, h, 1])
            linear = linear.astype(jnp.bfloat16).astype(jnp.float32)
            gated = gated.astype(jnp.bfloat16).astype(jnp.float32)
            small = smalls[h]
            act = jax.nn.gelu(conv_rows(gated, small) + small[3:4], approximate=True)
            hidden.append((act * linear).astype(jnp.bfloat16))
        for j in range(n_fs):
            total = dot_nn(hidden[0], ffn_all[j, 0, 2]) + dot_nn(hidden[1], ffn_all[j, second, 2])
            pf[i, s, :, j * width : (j + 1) * width] = total.astype(jnp.bfloat16)
        rs_core[i, s] = send(pf.at[i, s, theirs], rf.at[i, s], rs_s.at[0, i, s], rs_r.at[0, i, s], core)
        start(rs_core[i, s])

    def stage_core(i, s):
        wait(rs_core[i, s], f"rscore_{i}_{s}")
        total = pf[i, s, mine].astype(jnp.float32) + rf[i, s].astype(jnp.float32)
        sf[i, s] = total.astype(jnp.bfloat16)
        if s:
            rs_pair[i] = send(sf.at[i, s], rx.at[i], rs_s.at[1, i, 0], rs_r.at[1, i, 0], partner[i])
            start(rs_pair[i])

    def stage_pair(i):
        wait(rs_pair[i], f"rspair_{i}")
        total = (sf[i, 0].astype(jnp.float32) + rx[i].astype(jnp.float32)).astype(jnp.bfloat16)
        tf[i] = total
        if i > 0:
            rs_z[i] = send(tf.at[i], rz.at[f], rz_s.at[i], rz_r.at[f], {"fs": places[i]})
            start(rs_z[i])

    spread(0)
    forward(3)
    spread(1)
    pass_on(0)
    for i in range(1, 4):
        for p in range(3):
            wait(fy[i - 1][p], f"ffny_{i}_{p}")
    for i in range(4):
        for p in range(3):
            wait(fx[i][p], f"ffnx_{i}_{p}")
    wait(small_copy, "small")
    block(0, 0)
    block(0, 1)
    spread(2)
    pass_on(1)
    stage_core(0, 1)
    stage_core(0, 0)
    block(1, 0)
    block(1, 1)
    spread(3)
    pass_on(2)
    stage_core(1, 1)
    stage_core(1, 0)
    stage_pair(0)
    block(2, 0)
    block(2, 1)
    pass_on(3)
    stage_core(2, 1)
    stage_core(2, 0)
    stage_pair(1)
    block(3, 0)
    block(3, 1)
    stage_core(3, 1)
    stage_core(3, 0)
    stage_pair(2)
    stage_pair(3)

    total = tf[0].astype(jnp.float32)
    for i in range(1, 4):
        ref = rz.at[places[i]]
        wait(send(ref, ref, rz_s.at[0], rz_r.at[places[i]], {"fs": places[i]}), f"rz_{i}")
        total = total + rz[places[i]].astype(jnp.float32)
    branch = total.astype(jnp.bfloat16).astype(jnp.float32)
    done = middle[...].astype(jnp.float32) + norm_rows(branch, gain_ffn_post[...][None])
    out[slot] = done.astype(jnp.bfloat16)

    def row_slot(who):
        return out.at[pl.ds(pl.multiple_of(who * share, share), share)]

    own, far = row_slot(t), row_slot(t_side)
    fin_side = send(own, own, fin_s.at[0], fin_r.at[0], side)
    start(fin_side)
    fin_core = send(own, own, fin_s.at[1], fin_r.at[1], core)
    start(fin_core)
    wait(fin_side, "finside")
    fin_pass = send(far, far, fin_s.at[2], fin_r.at[2], core)
    start(fin_pass)
    wait(fin_core, "fincore")
    wait(fin_pass, "finpass")

    with scope("sends"):
        for copy, when in started:
            if when is None:
                copy.wait_send()
            else:
                pl.when(when)(copy.wait_send)


def split_plan(
    n_fs,
    stream,
    mix_pre_gain,
    w_outer_gate,
    w_inner_gate,
    w_value,
    mix_taps,
    w_mix_out,
    mix_post_gain,
    ffn_pre_gain,
    w_linear,
    w_gated,
    ffn_taps,
    ffn_bias,
    w_down,
    ffn_post_gain,
):
    rows, model = stream.shape
    width, conv_w = w_value.shape
    units = w_linear.shape[1] // n_fs
    low = units // 2 // PACK * PACK
    cap = -(-(units - low) // PACK) * PACK
    cut = lambda rows_of: rows_of.reshape(n_fs, units, width)
    share = rows // 4
    half = jnp.bfloat16
    vmem, dma = pltpu.VMEM, pltpu.SemaphoreType.DMA
    return pl.pallas_call(
        functools.partial(kernel, n_fs, conv_w, low, cap),
        out_shape=jax.ShapeDtypeStruct((rows, model), half),
        in_specs=[pl.BlockSpec(memory_space=vmem)] * 15,
        out_specs=pl.BlockSpec(memory_space=vmem),
        scratch_shapes=[
            vmem((n_fs, 2, 8, cap), jnp.float32),
            vmem((3, 8, cap), jnp.float32),
            vmem((n_fs, 3, cap, width), half),
            vmem((n_fs, 3, 3, cap, width), half),
            vmem((n_fs, 4 * conv_w, width), half),
            vmem((rows, model), half),
            vmem((2, SEQ_LEN, model), half),
            vmem((2, share, model), half),
            vmem((share, model), half),
            vmem((share, model), half),
            vmem((share, model), half),
            vmem((n_fs, 2, SEQ_LEN, model), half),
            vmem((n_fs, 2, SEQ_LEN, model), half),
            vmem((n_fs, 2, share, model), half),
            vmem((n_fs, 2, share, model), half),
            vmem((n_fs, share, model), half),
            vmem((n_fs, share, model), half),
            vmem((n_fs, share, model), half),
            dma((5 * CHUNKS,)),
            dma((n_fs, CHUNKS)),
            dma((3 * CHUNKS,)),
            dma((3 * CHUNKS,)),
            dma((3,)),
            dma((3,)),
            dma((3, 3)),
            dma((n_fs, 3)),
            dma((3, 3)),
            dma((3, 3)),
            dma((5, 3)),
            dma((5, 3)),
            dma((5, SPREAD)),
            dma((n_fs, SPREAD)),
            dma((3, n_fs, SPREAD)),
            dma((3, n_fs, SPREAD)),
            dma((2, n_fs, 2)),
            dma((2, n_fs, 2)),
            dma((n_fs,)),
            dma((n_fs,)),
            dma((3,)),
            dma((3,)),
        ],
        compiler_params=pltpu.CompilerParams(
            collective_id=0, has_side_effects=True, vmem_limit_bytes=56 * 2**20
        ),
    )(
        stream,
        mix_pre_gain,
        mix_post_gain,
        ffn_pre_gain,
        ffn_post_gain,
        w_outer_gate.T,
        w_inner_gate.T,
        w_value.T,
        w_mix_out,
        mix_taps,
        cut(w_linear.T),
        cut(w_gated.T),
        cut(w_down),
        ffn_taps,
        ffn_bias,
    )


def on_device(rep, n_fs, n_tp, *arrays):
    stream, w_value, w_linear = arrays[0], arrays[4], arrays[9]
    same = n_fs == n_tp == 2 * rep == 4
    whole = w_value.shape[0] % 128 == 0 and w_value.shape[1] % (CHUNKS * PACK) == 0
    even = w_linear.shape[1] % (8 * n_fs) == 0 and stream.shape[0] == 2 * SEQ_LEN
    if same and whole and even:
        return split_plan(n_fs, *arrays)
    return gather_plan(*arrays)


def solution(mesh):
    in_specs = (
        P(("rep", "fs"), None),
        P(),
        P("fs", "tp"),
        P("fs", "tp"),
        P("fs", "tp"),
        P(None, "tp"),
        P("tp", "fs"),
        P(),
        P(),
        P("fs", "tp"),
        P("fs", "tp"),
        P(None, "tp"),
        P("tp"),
        P("tp", "fs"),
        P(),
    )
    out_specs = P(("rep", "fs"), None)
    sizes = mesh.shape
    body = functools.partial(on_device, sizes["rep"], sizes["fs"], sizes["tp"])
    return jax.shard_map(
        body, mesh=mesh, in_specs=in_specs, out_specs=out_specs, check_vma=False
    )
```

time: 127 us -> 113 us (0.89)
  Pallas kernels: 124 us -> 111 us
    pallas_call x1, Pallas kernels: 124 us -> 111 us  [split_plan(): pl.pallas_call(functools.partial(kernel, n_fs, conv_w, low, cap), out_sha...]
where the time goes in v1:
time: 113 us
  Pallas kernels  111 us (98%)
  local copies, waits for them, and re-layouts  2.06 us (2%)
    pallas_call x1, Pallas kernels, split_plan(): pl.pallas_call(functools.partial(kernel, n_fs, conv_w, low, cap), out_sha...  111 us

profile of v1, /device:TPU:0, one launch (start us, length us, event | category | flops | bytes accessed | tf_op | source)
XLA Modules:
  0.0 112.6 jit_solution(5968693918452465508)
XLA Ops:
  0.0 110.5 %shard_map.145 = bf16[256,1536]{1,0:T(8,128)(2,1)} custom-call(bf16[256,1536]{1,0:T(8,128)(2,1)} %stream.1, f32[1536]{0:T(1024)} %gain_mix_pre.1, f32[1536]{0:T(1024)} %gain_mix_post.1, f32[1536]{0:T(1024)} %gain_ffn_pre.1, f32[1536]{0:T(1024)} %gain_ffn_post.1, bf16[192,384]{1,0:T(8,128)(2,1)} %bitcast.13, bf16[192,384]{1,0:T(8,128)(2,1)} %bitcast.14, ...), custom_call_target="tpu_custom_call" | custom-call | tf_op jit(solution)/shard_map/pallas_call | solution.py:565
  110.5 2.1 %copy.17 = bf16[256,1536]{1,0:T(8,128)(2,1)} copy(bf16[256,1536]{1,0:T(8,128)(2,1)} %shard_map.145) | data formatting | bytes 1572864

commit v2 on v1

--- a/solution.py
+++ b/solution.py
@@ -10,8 +10,20 @@
 
 SEQ_LEN = 128
 PACK = 16
-CHUNKS = 2
+CHUNKS = 4
 SPREAD = 2
+PARTS = 2
+EDGE = (
+    (),
+    ((3, 0), (3, 1), (3, 2), (1, 0)),
+    ((1, 1), (1, 2), (2, 0), (2, 1), (2, 2)),
+)
+INNER = (
+    ((1, 0), (1, 1), (1, 2)),
+    ((3, 0), (3, 1), (3, 2)),
+    ((2, 0), (2, 1), (2, 2)),
+)
+SIDEWAYS = (False, True, False, True)
 TRACE = False
 
 
@@ -114,73 +126,70 @@
     return jax.named_scope(name) if TRACE else contextlib.nullcontext()
 
 
-def kernel(
-    n_fs,
-    conv_w,
-    low,
-    cap,
-    stream,
-    gain_mix_pre,
-    gain_mix_post,
-    gain_ffn_pre,
-    gain_ffn_post,
-    w_outer,
-    w_inner,
-    w_value,
-    w_mix_out,
-    mix_taps,
-    w_linear,
-    w_gated,
-    w_down,
-    ffn_taps,
-    ffn_bias,
-    out,
-    small_all,
-    smalls,
-    ffn_w,
-    ffn_all,
-    mix_all,
-    normed,
-    pm,
-    rm,
-    sm,
-    rxm,
-    middle,
-    xs,
-    pf,
-    rf,
-    sf,
-    rx,
-    tf,
-    rz,
-    mz_s,
-    mz_r,
-    my_s,
-    my_r,
-    mr_s,
-    mr_r,
-    fz_s,
-    fz_r,
-    fy_s,
-    fy_r,
-    fx_s,
-    fx_r,
-    az_s,
-    az_r,
-    ap_s,
-    ap_r,
-    rs_s,
-    rs_r,
-    rz_s,
-    rz_r,
-    fin_s,
-    fin_r,
-):
+def kernel(n_fs, conv_w, low, cap, *refs):
+    sources, out, scratch = refs[:15], refs[15], refs[16:]
+    (
+        stream,
+        gain_mix_pre,
+        gain_mix_post,
+        gain_ffn_pre,
+        gain_ffn_post,
+        mix_taps,
+        w_linear,
+        w_gated,
+        w_down,
+        ffn_taps,
+        ffn_bias,
+        load_s,
+        small_all,
+        smalls,
+        ffn_w,
+        ffn_all,
+        mix_all,
+        normed,
+        acc,
+        pm,
+        rm,
+        sm,
+        rxm,
+        middle,
+        xs,
+        pf,
+        rf,
+        sf,
+        rx,
+        tf,
+        rz,
+        mz_s,
+        mz_r,
+        my_s,
+        my_r,
+        mr_s,
+        mr_r,
+        fz_s,
+        fz_r,
+        fy_s,
+        fy_r,
+        fx_s,
+        fx_r,
+        az_s,
+        az_r,
+        ap_s,
+        ap_r,
+        rs_s,
+        rs_r,
+        rp_s,
+        rp_r,
+        rz_s,
+        rz_r,
+        fin_s,
+        fin_r,
+    ) = scratch
     r, f, t = lax.axis_index("rep"), lax.axis_index("fs"), lax.axis_index("tp")
     x, c = t // 2, t % 2
     t_core, t_side = 2 * x + 1 - c, 2 * (1 - x) + c
     core, side, other = {"tp": t_core}, {"tp": t_side}, {"rep": 1 - r}
-    rows, width = stream.shape[0], w_value.shape[1]
+    rows, width = stream.shape[0], ffn_w.shape[3]
     units = w_linear.shape[1]
     share = rows // 4
     mine = pl.ds(pl.multiple_of(c * share, share), share)
@@ -215,6 +224,15 @@
         else:
             pl.when(when)(copy.start)
 
+    def flush(count=None):
+        with scope("sends"):
+            for copy, when in started[:count]:
+                if when is None:
+                    copy.wait_send()
+                else:
+                    pl.when(when)(copy.wait_send)
+        del started[:count]
+
     def wait(copy, name):
         with scope(name):
             copy.wait_recv()
@@ -223,8 +241,15 @@
     peers = [core, side, other] + [{"fs": (f + k) % n_fs} for k in (1, 2, 3)]
     for peer in peers:
         pl.semaphore_signal(barrier, inc=1, device_id=peer, device_id_type=pl.DeviceIdType.MESH)
-    for p, piece in enumerate((w_outer, w_inner, w_value, w_mix_out)):
-        mix_all[f, p * conv_w : (p + 1) * conv_w] = piece[...]
+    targets = [mix_all.at[f, p * conv_w : (p + 1) * conv_w] for p in range(4)]
+    targets += [stream, gain_mix_pre, w_linear, w_gated, w_down, ffn_taps, ffn_bias]
+    targets += [gain_mix_post, gain_ffn_pre, gain_ffn_post, mix_taps]
+    places_in = (5, 6, 7, 8, 0, 1, 10, 11, 12, 13, 14, 2, 3, 4, 9)
+    loads = [pltpu.make_async_copy(sources[i], ref, load_s.at[i]) for i, ref in zip(places_in, targets)]
+    for load in loads:
+        load.start()
+    for load in loads[:4]:
+        load.wait()
     with scope("barrier"):
         pl.semaphore_wait(barrier, len(peers))
 
@@ -239,6 +264,9 @@
     for h in range(CHUNKS):
         start(mix_copy(f, h, h, upward))
         start(mix_copy(f, h, CHUNKS + h, downward), inner)
+
+    for load in loads[6:]:
+        load.wait()
 
     for p, piece in enumerate((w_linear, w_gated, w_down)):
         for j in range(n_fs):
@@ -301,12 +329,23 @@
     small_copy = send(smalls.at[0], smalls.at[2], fx_s.at[4, 0], fx_r.at[4, 0], side)
     start(small_copy)
 
+    for load in loads[4:6]:
+        load.wait()
     step_rows = 32
 
     @pl.loop(0, rows // step_rows)
     def _(i):
         at = pl.ds(pl.multiple_of(i * step_rows, step_rows), step_rows)
-        normed[at] = norm_rows(stream[at].astype(jnp.float32), gain_mix_pre[...][None]).astype(jnp.bfloat16)
+        value = norm_rows(stream[at].astype(jnp.float32), gain_mix_pre[...][None]).astype(jnp.bfloat16)
+        for j in range(n_fs):
+            normed[j, at] = value[:, j * width : (j + 1) * width]
+
+    def project(z, first=False):
+        for p in range(3):
+            term = dot_nt(normed[z], mix_all[z, p * conv_w : (p + 1) * conv_w])
+            acc[p] = term if first else acc[p] + term
+
+    project(f, True)
 
     flows = [(i, h) for i in range(3) for h in range(CHUNKS)]
     turns = [(i, h) for h in range(CHUNKS) for i in range(2)] + [(2, h) for h in range(CHUNKS)]
@@ -334,35 +373,33 @@
             src, dst = ffn_all.at[places[i], 0, p], ffn_all.at[places[i], 1, p]
             fy[-1].append(send(src, dst, fy_s.at[i - 1, p], fy_r.at[i - 1, p], other))
 
-    def forward(i):
-        for p in range(3):
+    def forward(*which):
+        for i, p in which:
             src = ffn_all.at[places[i], 0, p]
             wait(send(src, src, fz_s.at[i - 1, p], fz_r.at[places[i], p], other), f"ffnz_{i}_{p}")
             fy[i - 1][p].start()
             fx[i][p].start()
 
+    def relay(edge_list, inner_list):
+        pl.when(edge)(functools.partial(forward, *edge_list))
+        pl.when(inner)(functools.partial(forward, *inner_list))
+
     for i in range(1, 4):
         started.extend((copy, None) for copy in fy[i - 1])
         started.extend((copy, None) for copy in fx[i])
 
-    @pl.when(inner)
-    def _():
-        forward(1)
-
+    relay(EDGE[0], INNER[0])
     for e in range(3 * CHUNKS):
         wait(my[e], f"mixy_{e}")
+        if e == 2 * CHUNKS - 1:
+            project(order[0])
+            project(order[1])
+    project(order[2])
 
     mix_core = []
     for k, q in enumerate((1 - x, x)):
         here = pl.ds(pl.multiple_of(q * SEQ_LEN, SEQ_LEN), SEQ_LEN)
-        parts = []
-        for p in range(3):
-            total = 0.0
-            for j in range(n_fs):
-                total = total + dot_nt(
-                    normed[here, j * width : (j + 1) * width], mix_all[j, p * conv_w : (p + 1) * conv_w]
-                )
-            parts.append(total.astype(jnp.bfloat16).astype(jnp.float32))
+        parts = [acc[p, here].astype(jnp.bfloat16).astype(jnp.float32) for p in range(3)]
         mixed = (parts[0] * conv_rows(parts[1] * parts[2], mix_taps)).astype(jnp.bfloat16)
         for j in range(n_fs):
             pm[k, :, j * width : (j + 1) * width] = dot_nn(
@@ -379,12 +416,8 @@
     mix_side = send(sm, rxm, mr_s.at[2], mr_r.at[2], side)
     start(mix_side)
 
-    @pl.when(edge)
-    def _():
-        forward(1)
-
     kept = mix_sum(1)
-    forward(2)
+    relay(EDGE[1], INNER[1])
     wait(mix_side, "mixside")
     branch = (kept.astype(jnp.float32) + rxm[...].astype(jnp.float32)).astype(jnp.bfloat16)
     slot = pl.ds(pl.multiple_of(t * share, share), share)
@@ -393,8 +426,7 @@
     middle[...] = mid
     xs[f, 0, mine] = norm_rows(mid.astype(jnp.float32), gain_ffn_pre[...][None]).astype(jnp.bfloat16)
 
-    across = [z % 2 == 0 for z in places]
-    partner = [{"rep": jnp.where(a, r, 1 - r), "tp": jnp.where(a, t_side, t)} for a in across]
+    partner = [side if SIDEWAYS[i] else other for i in range(4)]
     cut = share // SPREAD
 
     def piece_of(z, s, a):
@@ -427,12 +459,13 @@
             start(ag_pass[i, a])
 
     rs_core, rs_pair, rs_z = {}, {}, {}
+    part = share // PARTS
 
     def block(i, s):
         for a in range(SPREAD):
             wait((ag_pass if s else ag_core)[i, a], f"agcore_{i}_{s}_{a}")
         z = places[i]
-        second = jnp.where(across[i], 1, 2)
+        second = 1 if SIDEWAYS[i] else 2
         hidden = []
         for h in (0, second):
             linear, gated = 0.0, 0.0
@@ -453,24 +486,29 @@
 
     def stage_core(i, s):
         wait(rs_core[i, s], f"rscore_{i}_{s}")
-        total = pf[i, s, mine].astype(jnp.float32) + rf[i, s].astype(jnp.float32)
-        sf[i, s] = total.astype(jnp.bfloat16)
-        if s:
-            rs_pair[i] = send(sf.at[i, s], rx.at[i], rs_s.at[1, i, 0], rs_r.at[1, i, 0], partner[i])
-            start(rs_pair[i])
+        for a in range(PARTS):
+            at = pl.ds(a * part, part)
+            ours = pl.ds(pl.multiple_of(c * share + a * part, part), part)
+            total = pf[i, s, ours].astype(jnp.float32) + rf[i, s, at].astype(jnp.float32)
+            sf[i, s, at] = total.astype(jnp.bfloat16)
+            if s:
+                rs_pair[i, a] = send(sf.at[i, s, at], rx.at[i, at], rp_s.at[i, a], rp_r.at[i, a], partner[i])
+                start(rs_pair[i, a])
 
     def stage_pair(i):
-        wait(rs_pair[i], f"rspair_{i}")
-        total = (sf[i, 0].astype(jnp.float32) + rx[i].astype(jnp.float32)).astype(jnp.bfloat16)
-        tf[i] = total
-        if i > 0:
-            rs_z[i] = send(tf.at[i], rz.at[f], rz_s.at[i], rz_r.at[f], {"fs": places[i]})
-            start(rs_z[i])
+        for a in range(PARTS):
+            at = pl.ds(a * part, part)
+            wait(rs_pair[i, a], f"rspair_{i}_{a}")
+            tf[i, at] = (sf[i, 0, at].astype(jnp.float32) + rx[i, at].astype(jnp.float32)).astype(jnp.bfloat16)
+            if i > 0:
+                copy = send(tf.at[i, at], rz.at[f, at], rz_s.at[i, a], rz_r.at[f, a], {"fs": places[i]})
+                start(copy)
 
     spread(0)
-    forward(3)
+    relay(EDGE[2], INNER[2])
+    pass_on(0)
     spread(1)
-    pass_on(0)
+    spread(2)
     for i in range(1, 4):
         for p in range(3):
             wait(fy[i - 1][p], f"ffny_{i}_{p}")
@@ -479,60 +517,60 @@
             wait(fx[i][p], f"ffnx_{i}_{p}")
     wait(small_copy, "small")
     block(0, 0)
+    pass_on(1)
     block(0, 1)
-    spread(2)
-    pass_on(1)
+    block(1, 0)
     stage_core(0, 1)
     stage_core(0, 0)
-    block(1, 0)
+    spread(3)
     block(1, 1)
-    spread(3)
     pass_on(2)
+    block(2, 0)
+    early = len(started)
     stage_core(1, 1)
     stage_core(1, 0)
+    block(2, 1)
     stage_pair(0)
-    block(2, 0)
-    block(2, 1)
+    block(3, 0)
     pass_on(3)
     stage_core(2, 1)
     stage_core(2, 0)
+    block(3, 1)
     stage_pair(1)
-    block(3, 0)
-    block(3, 1)
     stage_core(3, 1)
     stage_core(3, 0)
     stage_pair(2)
+    flush(early)
     stage_pair(3)
 
-    total = tf[0].astype(jnp.float32)
-    for i in range(1, 4):
-        ref = rz.at[places[i]]
-        wait(send(ref, ref, rz_s.at[0], rz_r.at[places[i]], {"fs": places[i]}), f"rz_{i}")
-        total = total + rz[places[i]].astype(jnp.float32)
-    branch = total.astype(jnp.bfloat16).astype(jnp.float32)
-    done = middle[...].astype(jnp.float32) + norm_rows(branch, gain_ffn_post[...][None])
-    out[slot] = done.astype(jnp.bfloat16)
-
-    def row_slot(who):
-        return out.at[pl.ds(pl.multiple_of(who * share, share), share)]
-
-    own, far = row_slot(t), row_slot(t_side)
-    fin_side = send(own, own, fin_s.at[0], fin_r.at[0], side)
-    start(fin_side)
-    fin_core = send(own, own, fin_s.at[1], fin_r.at[1], core)
-    start(fin_core)
-    wait(fin_side, "finside")
-    fin_pass = send(far, far, fin_s.at[2], fin_r.at[2], core)
-    start(fin_pass)
-    wait(fin_core, "fincore")
-    wait(fin_pass, "finpass")
-
-    with scope("sends"):
-        for copy, when in started:
-            if when is None:
-                copy.wait_send()
-            else:
-                pl.when(when)(copy.wait_send)
+    def row_slot(who, a):
+        return pl.ds(pl.multiple_of(who * share + a * part, part), part)
+
+    fin = {}
+    for a in range(PARTS):
+        at = pl.ds(a * part, part)
+        total = tf[0, at].astype(jnp.float32)
+        for i in range(1, 4):
+            ref = rz.at[places[i], at]
+            wait(send(ref, ref, rz_s.at[0, a], rz_r.at[places[i], a], {"fs": places[i]}), f"rz_{i}_{a}")
+            total = total + rz[places[i], at].astype(jnp.float32)
+        branch = total.astype(jnp.bfloat16).astype(jnp.float32)
+        done = middle[at].astype(jnp.float32) + norm_rows(branch, gain_ffn_post[...][None])
+        out[row_slot(t, a)] = done.astype(jnp.bfloat16)
+        own = out.at[row_slot(t, a)]
+        for k, to in enumerate((side, core)):
+            fin[k, a] = send(own, own, fin_s.at[k, a], fin_r.at[k, a], to)
+            start(fin[k, a])
+    for a in range(PARTS):
+        wait(fin[0, a], f"finside_{a}")
+        far = out.at[row_slot(t_side, a)]
+        fin[2, a] = send(far, far, fin_s.at[2, a], fin_r.at[2, a], core)
+        start(fin[2, a])
+    for a in range(PARTS):
+        wait(fin[1, a], f"fincore_{a}")
+        wait(fin[2, a], f"finpass_{a}")
+
+    flush()
 
 
 def split_plan(
@@ -565,15 +603,28 @@
     return pl.pallas_call(
         functools.partial(kernel, n_fs, conv_w, low, cap),
         out_shape=jax.ShapeDtypeStruct((rows, model), half),
-        in_specs=[pl.BlockSpec(memory_space=vmem)] * 15,
+        in_specs=[pl.BlockSpec(memory_space=pl.ANY)] * 15,
         out_specs=pl.BlockSpec(memory_space=vmem),
         scratch_shapes=[
+            vmem((rows, model), half),
+            vmem((model,), jnp.float32),
+            vmem((model,), jnp.float32),
+            vmem((model,), jnp.float32),
+            vmem((model,), jnp.float32),
+            vmem(mix_taps.shape, jnp.float32),
+            vmem((n_fs, units, width), half),
+            vmem((n_fs, units, width), half),
+            vmem((n_fs, units, width), half),
+            vmem(ffn_taps.shape, jnp.float32),
+            vmem(ffn_bias.shape, jnp.float32),
+            dma((15,)),
             vmem((n_fs, 2, 8, cap), jnp.float32),
             vmem((3, 8, cap), jnp.float32),
             vmem((n_fs, 3, cap, width), half),
             vmem((n_fs, 3, 3, cap, width), half),
             vmem((n_fs, 4 * conv_w, width), half),
-            vmem((rows, model), half),
+            vmem((n_fs, rows, width), half),
+            vmem((3, rows, conv_w), jnp.float32),
             vmem((2, SEQ_LEN, model), half),
             vmem((2, share, model), half),
             vmem((share, model), half),
@@ -602,12 +653,14 @@
             dma((n_fs, SPREAD)),
             dma((3, n_fs, SPREAD)),
             dma((3, n_fs, SPREAD)),
-            dma((2, n_fs, 2)),
-            dma((2, n_fs, 2)),
-            dma((n_fs,)),
-            dma((n_fs,)),
-            dma((3,)),
-            dma((3,)),
+            dma((1, n_fs, 2)),
+            dma((1, n_fs, 2)),
+            dma((n_fs, PARTS)),
+            dma((n_fs, PARTS)),
+            dma((n_fs, PARTS)),
+            dma((n_fs, PARTS)),
+            dma((3, PARTS)),
+            dma((3, PARTS)),
         ],
         compiler_params=pltpu.CompilerParams(
             collective_id=0, has_side_effects=True, vmem_limit_bytes=56 * 2**20
@@ -634,7 +687,7 @@
 def on_device(rep, n_fs, n_tp, *arrays):
     stream, w_value, w_linear = arrays[0], arrays[4], arrays[9]
     same = n_fs == n_tp == 2 * rep == 4
-    whole = w_value.shape[0] % 128 == 0 and w_value.shape[1] % (CHUNKS * PACK) == 0
+    whole = w_value.shape[0] % 128 == 0 and 2 * w_value.shape[1] % (CHUNKS * PACK) == 0
     even = w_linear.shape[1] % (8 * n_fs) == 0 and stream.shape[0] == 2 * SEQ_LEN
     if same and whole and even:
         return split_plan(n_fs, *arrays)

time: 113 us -> 102 us (0.903)
  Pallas kernels: 111 us -> 99.6 us
    pallas_call x1, Pallas kernels: 111 us -> 99.6 us  [split_plan(): pl.pallas_call(functools.partial(kernel, n_fs, conv_w, low, cap), out_sha...]
where the time goes in v2:
time: 102 us
  Pallas kernels  99.6 us (98%)
  local copies, waits for them, and re-layouts  2.06 us (2%)
    pallas_call x1, Pallas kernels, split_plan(): pl.pallas_call(functools.partial(kernel, n_fs, conv_w, low, cap), out_sha...  99.6 us
    unnamed x1, local copies, waits for them, and re-layouts  2.06 us

profile of v2, /device:TPU:0, one launch (start us, length us, event | category | flops | bytes accessed | tf_op | source)
XLA Modules:
  0.0 101.6 jit_solution(14539934381085047677)
XLA Ops:
  0.0 99.6 %shard_map.145 = bf16[256,1536]{1,0:T(8,128)(2,1)} custom-call(bf16[256,1536]{1,0:T(8,128)(2,1)} %refs_0_.1, f32[1536]{0:T(1024)} %refs_1_.1, f32[1536]{0:T(1024)} %refs_2_.1, f32[1536]{0:T(1024)} %refs_3_.1, f32[1536]{0:T(1024)} %refs_4_.1, bf16[192,384]{1,0:T(8,128)(2,1)} %bitcast.13, bf16[192,384]{1,0:T(8,128)(2,1)} %bitcast.14, ...), custom_call_target="tpu_custom_call" | custom-call | tf_op jit(solution)/shard_map/pallas_call | solution.py:603
  99.6 2.1 %copy.17 = bf16[256,1536]{1,0:T(8,128)(2,1)} copy(bf16[256,1536]{1,0:T(8,128)(2,1)} %shard_map.145) | data formatting | bytes 1572864

commit v3 on v2

--- a/solution.py
+++ b/solution.py
@@ -12,18 +12,20 @@
 PACK = 16
 CHUNKS = 4
 SPREAD = 2
-PARTS = 2
+PARTS = 4
+JOIN = 2
 EDGE = (
+    (),
     (),
     ((3, 0), (3, 1), (3, 2), (1, 0)),
     ((1, 1), (1, 2), (2, 0), (2, 1), (2, 2)),
 )
 INNER = (
     ((1, 0), (1, 1), (1, 2)),
+    (),
     ((3, 0), (3, 1), (3, 2)),
     ((2, 0), (2, 1), (2, 2)),
 )
-SIDEWAYS = (False, True, False, True)
 TRACE = False
 
 
@@ -126,7 +128,7 @@
     return jax.named_scope(name) if TRACE else contextlib.nullcontext()
 
 
-def kernel(n_fs, conv_w, low, cap, *refs):
+def kernel(n_fs, conv_w, spans, *refs):
     sources, out, scratch = refs[:15], refs[15], refs[16:]
     (
         stream,
@@ -160,6 +162,7 @@
         rx,
         tf,
         rz,
+        rq,
         mz_s,
         mz_r,
         my_s,
@@ -182,6 +185,7 @@
         rp_r,
         rz_s,
         rz_r,
+        rq_r,
         fin_s,
         fin_r,
     ) = scratch
@@ -190,11 +194,11 @@
     t_core, t_side = 2 * x + 1 - c, 2 * (1 - x) + c
     core, side, other = {"tp": t_core}, {"tp": t_side}, {"rep": 1 - r}
     rows, width = stream.shape[0], ffn_w.shape[3]
-    units = w_linear.shape[1]
+    cap, few = ffn_w.shape[2], spans[0][1]
+    sizes = (few, cap)
     share = rows // 4
     mine = pl.ds(pl.multiple_of(c * share, share), share)
     theirs = pl.ds(pl.multiple_of((1 - c) * share, share), share)
-    high = units - low
 
     near = f < n_fs // 2
     mirror = lambda v: jnp.where(near, v, n_fs - 1 - v)
@@ -268,60 +272,63 @@
     for load in loads[6:]:
         load.wait()
 
-    for p, piece in enumerate((w_linear, w_gated, w_down)):
-        for j in range(n_fs):
-            ffn_w[j, p, low:cap] = jnp.zeros((cap - low, width), ffn_w.dtype)
-
-        @pl.when(r == 0)
+    pieces = (w_linear, w_gated, w_down)
+
+    def keep(ref, at, size, piece):
+        ref[0:size] = piece[at : at + size]
+        if size < cap:
+            ref[size:cap] = jnp.zeros((cap - size, width), ffn_w.dtype)
+
+    for half in range(2):
+
+        @pl.when(r == half)
         def _():
-            for j in range(n_fs):
-                ffn_w[j, p, 0:low] = piece[j, 0:low]
-
-        @pl.when(r == 1)
-        def _():
-            for j in range(n_fs):
-                ffn_w[j, p, 0:high] = piece[j, low:units]
-
-    def ffn_send(i):
+            for j, (at, *both) in enumerate(spans):
+                for p, piece in enumerate(pieces):
+                    keep(ffn_w.at[j, p], at + half * both[0], both[half], piece)
+
+    narrow = ((cap, cap, few), (cap, few, few))
+
+    def ffn_send(kind, i):
         for p in range(3):
-            src, dst = ffn_w.at[goals[i], p], ffn_all.at[f, 0, p]
+            at = slice(0, narrow[kind][i])
+            src, dst = ffn_w.at[goals[i], p, at], ffn_all.at[f, 0, p, at]
             yield send(src, dst, fz_s.at[i, p], fz_r.at[f, p], {"fs": goals[i]})
 
-    ffn_out = [list(ffn_send(i)) for i in range(3)]
-    started += [(copy, None) for copies in ffn_out for copy in copies]
-
-    def ffn_start(*which):
+    kinds = (edge, inner)
+    ffn_out = [[list(ffn_send(kind, i)) for i in range(3)] for kind in range(2)]
+    for kind in range(2):
+        started.extend((copy, kinds[kind]) for copies in ffn_out[kind] for copy in copies)
+
+    def ffn_start(kind, *which):
         for i in which:
-            for copy in ffn_out[i]:
+            for copy in ffn_out[kind][i]:
                 copy.start()
 
-    pl.when(edge)(functools.partial(ffn_start, 0, 1, 2))
-
-    def ffn_side(i):
-        for p in range(3):
-            src = ffn_w.at[f, p] if i == 0 else ffn_all.at[places[i], 0, p]
-            dst = ffn_all.at[places[i], 2, p]
-            yield send(src, dst, fx_s.at[i, p], fx_r.at[i, p], side)
-
-    fx = [list(ffn_side(i)) for i in range(4)]
-    for copy in fx[0]:
+    pl.when(edge)(functools.partial(ffn_start, 0, 0, 1, 2))
+
+    own_side = [send(ffn_w.at[f, p], ffn_all.at[f, 2, p], fx_s.at[0, p], fx_r.at[0, p], side) for p in range(3)]
+    for copy in own_side:
         start(copy)
-    for p, piece in enumerate((w_linear, w_gated, w_down)):
+    for p in range(3):
         ffn_all[f, 0, p] = ffn_w[f, p]
-        ffn_all[f, 1, p, low:cap] = jnp.zeros((cap - low, width), ffn_w.dtype)
-
-        @pl.when(r == 0)
-        def _():
-            ffn_all[f, 1, p, 0:high] = piece[f, low:units]
-
-        @pl.when(r == 1)
-        def _():
-            ffn_all[f, 1, p, 0:low] = piece[f, 0:low]
+    for j, (at, *both) in enumerate(spans):
+        for half in range(2):
+
+            @pl.when((f == j) & (r == half))
+            def _():
+                for p, piece in enumerate(pieces):
+                    keep(ffn_all.at[j, 1, p], at + (1 - half) * both[0], both[1 - half], piece)
+
+    @pl.when(edge)
+    def _():
+        for i in range(1, 4):
+            ffn_all[places[i], :, :, few:cap] = jnp.zeros((3, 3, cap - few, width), ffn_w.dtype)
 
     small_all[...] = jnp.zeros(small_all.shape, jnp.float32)
-    for j in range(n_fs):
-        for half, size in enumerate((low, high)):
-            at = j * units + half * low
+    for j, (first, *both) in enumerate(spans):
+        for half, size in enumerate(both):
+            at = first + half * both[0]
             small_all[j, half, 0:3, 0:size] = ffn_taps[:, at : at + size]
             small_all[j, half, 3:4, 0:size] = ffn_bias[at : at + size][None]
     smalls[0] = small_all[f, r]
@@ -363,33 +370,42 @@
         my.append(send(ref, ref, my_s.at[e], my_r.at[e], other))
         start(my[e])
         if e == 2 * CHUNKS - 2:
-            pl.when(inner)(functools.partial(ffn_start, 0, 1))
-    pl.when(inner)(functools.partial(ffn_start, 2))
-
-    fy = []
-    for i in range(1, 4):
-        fy.append([])
-        for p in range(3):
-            src, dst = ffn_all.at[places[i], 0, p], ffn_all.at[places[i], 1, p]
-            fy[-1].append(send(src, dst, fy_s.at[i - 1, p], fy_r.at[i - 1, p], other))
-
-    def forward(*which):
+            pl.when(inner)(functools.partial(ffn_start, 1, 0, 1))
+    pl.when(inner)(functools.partial(ffn_start, 1, 2))
+
+    def hop(kind, i, p, piece, ss, rs, to):
+        src = ffn_all.at[places[i], 0, p, 0 : sizes[kind]]
+        dst = ffn_all.at[places[i], piece, p, 0 : sizes[kind]]
+        return send(src, dst, ss.at[i, p], rs.at[i, p], to)
+
+    trips = [(i, p) for i in range(1, 4) for p in range(3)]
+    fy = [{(i, p): hop(kind, i, p, 1, fy_s, fy_r, other) for i, p in trips} for kind in range(2)]
+    fx = [{(i, p): hop(kind, i, p, 2, fx_s, fx_r, side) for i, p in trips} for kind in range(2)]
+    for kind in range(2):
+        for group in (fy, fx):
+            started.extend((copy, kinds[kind]) for copy in group[kind].values())
+
+    def forward(kind, *which):
         for i, p in which:
-            src = ffn_all.at[places[i], 0, p]
+            src = ffn_all.at[places[i], 0, p, 0 : sizes[kind]]
             wait(send(src, src, fz_s.at[i - 1, p], fz_r.at[places[i], p], other), f"ffnz_{i}_{p}")
-            fy[i - 1][p].start()
-            fx[i][p].start()
+            fy[kind][i, p].start()
+            fx[kind][i, p].start()
 
     def relay(edge_list, inner_list):
-        pl.when(edge)(functools.partial(forward, *edge_list))
-        pl.when(inner)(functools.partial(forward, *inner_list))
-
-    for i in range(1, 4):
-        started.extend((copy, None) for copy in fy[i - 1])
-        started.extend((copy, None) for copy in fx[i])
+        for kind, which in enumerate((edge_list, inner_list)):
+            if which:
+                pl.when(kinds[kind])(functools.partial(forward, kind, *which))
+
+    def arrived(kind):
+        for i, p in trips:
+            wait(fy[kind][i, p], f"ffny_{i}_{p}")
+            wait(fx[kind][i, p], f"ffnx_{i}_{p}")
 
     relay(EDGE[0], INNER[0])
     for e in range(3 * CHUNKS):
+        if e == 3 * CHUNKS - 1:
+            relay(EDGE[1], INNER[1])
         wait(my[e], f"mixy_{e}")
         if e == 2 * CHUNKS - 1:
             project(order[0])
@@ -417,7 +433,7 @@
     start(mix_side)
 
     kept = mix_sum(1)
-    relay(EDGE[1], INNER[1])
+    relay(EDGE[2], INNER[2])
     wait(mix_side, "mixside")
     branch = (kept.astype(jnp.float32) + rxm[...].astype(jnp.float32)).astype(jnp.bfloat16)
     slot = pl.ds(pl.multiple_of(t * share, share), share)
@@ -426,7 +442,8 @@
     middle[...] = mid
     xs[f, 0, mine] = norm_rows(mid.astype(jnp.float32), gain_ffn_pre[...][None]).astype(jnp.bfloat16)
 
-    partner = [side if SIDEWAYS[i] else other for i in range(4)]
+    sideways = [edge == (i % 2 == 1) for i in range(4)]
+    partner = [{"rep": jnp.where(a, r, 1 - r), "tp": jnp.where(a, t_side, t)} for a in sideways]
     cut = share // SPREAD
 
     def piece_of(z, s, a):
@@ -434,55 +451,74 @@
 
     ag_core, ag_pair, ag_pass = {}, {}, {}
 
+    def line_copy(i, a):
+        src = piece_of(places[i], 0, a)
+        onward = downward if i > 1 else upward
+        return send(src, src, az_s.at[1 + i, a], az_r.at[places[i], a], {"fs": onward})
+
+    ag_line = {(i, a): line_copy(i, a) for i in range(1, 4) for a in range(SPREAD)}
+    for i in range(4):
+        for a in range(SPREAD):
+            src = piece_of(places[i], 0, a)
+            ag_pair[i, a] = send(src, piece_of(places[i], 1, a), ap_s.at[0, i, a], ap_r.at[0, i, a], partner[i])
+            ag_core[i, a] = send(src, src, ap_s.at[1, i, a], ap_r.at[1, i, a], core)
+            started.extend(((ag_pair[i, a], None), (ag_core[i, a], None)))
+            if i > 0:
+                started.append((ag_line[i, a], inner))
+
     def spread(i):
-        z = places[i]
         for a in range(SPREAD):
-            src = piece_of(z, 0, a)
+            src = piece_of(places[i], 0, a)
             if i == 0:
-                start(send(src, src, az_s.at[0, a], az_r.at[z, a], {"fs": upward}))
-                start(send(src, src, az_s.at[1, a], az_r.at[z, a], {"fs": downward}), inner)
+                start(send(src, src, az_s.at[0, a], az_r.at[places[i], a], {"fs": upward}))
+                start(send(src, src, az_s.at[1, a], az_r.at[places[i], a], {"fs": downward}), inner)
             else:
-                onward = downward if i > 1 else upward
-                copy = send(src, src, az_s.at[1 + i, a], az_r.at[z, a], {"fs": onward})
-                wait(copy, f"agz_{i}_{a}")
-                start(copy, inner)
-            ag_pair[i, a] = send(src, piece_of(z, 1, a), ap_s.at[0, i, a], ap_r.at[0, i, a], partner[i])
-            start(ag_pair[i, a])
-            ag_core[i, a] = send(src, src, ap_s.at[1, i, a], ap_r.at[1, i, a], core)
-            start(ag_core[i, a])
+                wait(ag_line[i, a], f"agz_{i}_{a}")
+                pl.when(inner)(ag_line[i, a].start)
+            ag_pair[i, a].start()
+            ag_core[i, a].start()
+
+    for i in range(4):
+        for a in range(SPREAD):
+            src = piece_of(places[i], 1, a)
+            ag_pass[i, a] = send(src, src, ap_s.at[2, i, a], ap_r.at[2, i, a], core)
+            started.append((ag_pass[i, a], None))
 
     def pass_on(i):
         for a in range(SPREAD):
             wait(ag_pair[i, a], f"agpair_{i}_{a}")
-            src = piece_of(places[i], 1, a)
-            ag_pass[i, a] = send(src, src, ap_s.at[2, i, a], ap_r.at[2, i, a], core)
-            start(ag_pass[i, a])
-
-    rs_core, rs_pair, rs_z = {}, {}, {}
+            ag_pass[i, a].start()
+
+    rs_core, rs_pair = {}, {}
     part = share // PARTS
 
-    def block(i, s):
-        for a in range(SPREAD):
-            wait((ag_pass if s else ag_core)[i, a], f"agcore_{i}_{s}_{a}")
+    def block(i):
+        for s in range(2):
+            for a in range(SPREAD):
+                wait((ag_pass if s else ag_core)[i, a], f"agcore_{i}_{s}_{a}")
         z = places[i]
-        second = 1 if SIDEWAYS[i] else 2
-        hidden = []
-        for h in (0, second):
-            linear, gated = 0.0, 0.0
+        second = jnp.where(sideways[i], 1, 2)
+        with scope(f"block_{i}"):
+            hidden = []
+            for h in (0, second):
+                linear, gated = 0.0, 0.0
+                for j in range(0, n_fs, JOIN):
+                    act = xs[z, :, :, j * width : (j + JOIN) * width].reshape(2 * SEQ_LEN, JOIN * width)
+                    joined = lambda p: jnp.concatenate([ffn_all[j + k, h, p] for k in range(JOIN)], axis=1)
+                    linear = linear + dot_nt(act, joined(0))
+                    gated = gated + dot_nt(act, joined(1))
+                linear = linear.astype(jnp.bfloat16).astype(jnp.float32)
+                gated = gated.astype(jnp.bfloat16).astype(jnp.float32)
+                small = smalls[h]
+                act = jax.nn.gelu(conv_rows(gated, small) + small[3:4], approximate=True)
+                hidden.append((act * linear).astype(jnp.bfloat16))
             for j in range(n_fs):
-                act = xs[z, s, :, j * width : (j + 1) * width]
-                linear = linear + dot_nt(act, ffn_all[j, h, 0])
-                gated = gated + dot_nt(act, ffn_all[j, h, 1])
-            linear = linear.astype(jnp.bfloat16).astype(jnp.float32)
-            gated = gated.astype(jnp.bfloat16).astype(jnp.float32)
-            small = smalls[h]
-            act = jax.nn.gelu(conv_rows(gated, small) + small[3:4], approximate=True)
-            hidden.append((act * linear).astype(jnp.bfloat16))
-        for j in range(n_fs):
-            total = dot_nn(hidden[0], ffn_all[j, 0, 2]) + dot_nn(hidden[1], ffn_all[j, second, 2])
-            pf[i, s, :, j * width : (j + 1) * width] = total.astype(jnp.bfloat16)
-        rs_core[i, s] = send(pf.at[i, s, theirs], rf.at[i, s], rs_s.at[0, i, s], rs_r.at[0, i, s], core)
-        start(rs_core[i, s])
+                total = dot_nn(hidden[0], ffn_all[j, 0, 2]) + dot_nn(hidden[1], ffn_all[j, second, 2])
+                total = total.astype(jnp.bfloat16).reshape(2, SEQ_LEN, width)
+                pf[i, :, :, j * width : (j + 1) * width] = total
+        for s in (1, 0):
+            rs_core[i, s] = send(pf.at[i, s, theirs], rf.at[i, s], rs_s.at[0, i, s], rs_r.at[0, i, s], core)
+            start(rs_core[i, s])
 
     def stage_core(i, s):
         wait(rs_core[i, s], f"rscore_{i}_{s}")
@@ -495,53 +531,96 @@
                 rs_pair[i, a] = send(sf.at[i, s, at], rx.at[i, at], rp_s.at[i, a], rp_r.at[i, a], partner[i])
                 start(rs_pair[i, a])
 
+    rs_line, late = {}, []
+    for i in range(1, 4):
+        for a in range(PARTS):
+            at = pl.ds(a * part, part)
+            home = send(tf.at[i, at], rz.at[f, at], rz_s.at[i, a], rz_r.at[f, a], {"fs": places[i]})
+            late.append((home, None if i == 1 else inner))
+            rs_line[i, a] = home, None
+            if i > 1:
+                near_by = send(tf.at[i, at], rq.at[i, at], rz_s.at[i, a], rq_r.at[i, a], {"fs": places[1]})
+                late.append((near_by, edge))
+                rs_line[i, a] = home, near_by
+
     def stage_pair(i):
         for a in range(PARTS):
             at = pl.ds(a * part, part)
             wait(rs_pair[i, a], f"rspair_{i}_{a}")
-            tf[i, at] = (sf[i, 0, at].astype(jnp.float32) + rx[i, at].astype(jnp.float32)).astype(jnp.bfloat16)
-            if i > 0:
-                copy = send(tf.at[i, at], rz.at[f, at], rz_s.at[i, a], rz_r.at[f, a], {"fs": places[i]})
-                start(copy)
+            total = sf[i, 0, at].astype(jnp.float32) + rx[i, at].astype(jnp.float32)
+            if i == 0:
+                tf[i, at] = total.astype(jnp.bfloat16)
+                continue
+            home, near_by = rs_line[i, a]
+            if near_by is None:
+                tf[i, at] = total.astype(jnp.bfloat16)
+                home.start()
+                continue
+
+            @pl.when(edge)
+            def _():
+                tf[i, at] = total.astype(jnp.bfloat16)
+                near_by.start()
+
+            @pl.when(inner)
+            def _():
+                wait(near_by, f"rq_{i}_{a}")
+                tf[i, at] = (total + rq[i, at].astype(jnp.float32)).astype(jnp.bfloat16)
+                home.start()
+
+    def stage(i):
+        stage_core(i, 1)
+        stage_core(i, 0)
 
     spread(0)
-    relay(EDGE[2], INNER[2])
-    pass_on(0)
-    spread(1)
-    spread(2)
-    for i in range(1, 4):
-        for p in range(3):
-            wait(fy[i - 1][p], f"ffny_{i}_{p}")
-    for i in range(4):
-        for p in range(3):
-            wait(fx[i][p], f"ffnx_{i}_{p}")
-    wait(small_copy, "small")
-    block(0, 0)
+    relay(EDGE[3], INNER[3])
+
+    @pl.when(edge)
+    def _():
+        pass_on(0)
+        spread(1)
+        spread(2)
+        arrived(0)
+
+    @pl.when(inner)
+    def _():
+        spread(1)
+        spread(2)
+        spread(3)
+        pass_on(0)
+        arrived(1)
+
+    for copy in own_side + [small_copy]:
+        wait(copy, "ffnown")
+    block(0)
     pass_on(1)
-    block(0, 1)
-    block(1, 0)
-    stage_core(0, 1)
-    stage_core(0, 0)
-    spread(3)
-    block(1, 1)
+    pl.when(edge)(functools.partial(spread, 3))
     pass_on(2)
-    block(2, 0)
     early = len(started)
-    stage_core(1, 1)
-    stage_core(1, 0)
-    block(2, 1)
+    block(1)
+    block(2)
+    stage(1)
+    pass_on(3)
+    stage(2)
+    stage(0)
+    block(3)
+    stage(3)
+
+    @pl.when(edge)
+    def _():
+        stage_pair(2)
+        stage_pair(3)
+        stage_pair(1)
+
+    @pl.when(inner)
+    def _():
+        stage_pair(1)
+        stage_pair(2)
+        stage_pair(3)
+
     stage_pair(0)
-    block(3, 0)
-    pass_on(3)
-    stage_core(2, 1)
-    stage_core(2, 0)
-    block(3, 1)
-    stage_pair(1)
-    stage_core(3, 1)
-    stage_core(3, 0)
-    stage_pair(2)
     flush(early)
-    stage_pair(3)
+    started.extend(late)
 
     def row_slot(who, a):
         return pl.ds(pl.multiple_of(who * share + a * part, part), part)
@@ -550,7 +629,7 @@
     for a in range(PARTS):
         at = pl.ds(a * part, part)
         total = tf[0, at].astype(jnp.float32)
-        for i in range(1, 4):
+        for i in range(1, 3):
             ref = rz.at[places[i], at]
             wait(send(ref, ref, rz_s.at[0, a], rz_r.at[places[i], a], {"fs": places[i]}), f"rz_{i}_{a}")
             total = total + rz[places[i], at].astype(jnp.float32)
@@ -593,17 +672,22 @@
 ):
     rows, model = stream.shape
     width, conv_w = w_value.shape
-    units = w_linear.shape[1] // n_fs
-    low = units // 2 // PACK * PACK
-    cap = -(-(units - low) // PACK) * PACK
-    cut = lambda rows_of: rows_of.reshape(n_fs, units, width)
+    tiles = w_linear.shape[1] // (2 * PACK)
+    few = tiles * 7 // 32 * PACK
+    more = tiles * PACK - 2 * few
+    cap = -(-more // (2 * PACK)) * PACK
+    spans, at = [], 0
+    for z in range(n_fs):
+        both = (few, few) if z in (0, n_fs - 1) else (cap, more - cap)
+        spans.append((at, *both))
+        at += sum(both)
     share = rows // 4
     half = jnp.bfloat16
     vmem, dma = pltpu.VMEM, pltpu.SemaphoreType.DMA
     return pl.pallas_call(
-        functools.partial(kernel, n_fs, conv_w, low, cap),
-        out_shape=jax.ShapeDtypeStruct((rows, model), half),
-        in_specs=[pl.BlockSpec(memory_space=pl.ANY)] * 15,
+        functools.partial(kernel, n_fs, conv_w, tuple(spans)),
+        out_shape=pltpu.VMEM((rows, model), half),
+        in_specs=[pl.BlockSpec(memory_space=pltpu.HBM)] * 15,
         out_specs=pl.BlockSpec(memory_space=vmem),
         scratch_shapes=[
             vmem((rows, model), half),
@@ -612,9 +696,9 @@
             vmem((model,), jnp.float32),
             vmem((model,), jnp.float32),
             vmem(mix_taps.shape, jnp.float32),
-            vmem((n_fs, units, width), half),
-            vmem((n_fs, units, width), half),
-            vmem((n_fs, units, width), half),
+            vmem(w_down.shape, half),
+            vmem(w_down.shape, half),
+            vmem(w_down.shape, half),
             vmem(ffn_taps.shape, jnp.float32),
             vmem(ffn_bias.shape, jnp.float32),
             dma((15,)),
@@ -637,6 +721,7 @@
             vmem((n_fs, share, model), half),
             vmem((n_fs, share, model), half),
             vmem((n_fs, share, model), half),
+            vmem((n_fs, share, model), half),
             dma((5 * CHUNKS,)),
             dma((n_fs, CHUNKS)),
             dma((3 * CHUNKS,)),
@@ -645,8 +730,8 @@
             dma((3,)),
             dma((3, 3)),
             dma((n_fs, 3)),
-            dma((3, 3)),
-            dma((3, 3)),
+            dma((n_fs, 3)),
+            dma((n_fs, 3)),
             dma((5, 3)),
             dma((5, 3)),
             dma((5, SPREAD)),
@@ -659,11 +744,12 @@
             dma((n_fs, PARTS)),
             dma((n_fs, PARTS)),
             dma((n_fs, PARTS)),
+            dma((n_fs, PARTS)),
             dma((3, PARTS)),
             dma((3, PARTS)),
         ],
         compiler_params=pltpu.CompilerParams(
-            collective_id=0, has_side_effects=True, vmem_limit_bytes=56 * 2**20
+            collective_id=0, has_side_effects=True, vmem_limit_bytes=58 * 2**20
         ),
     )(
         stream,
@@ -676,9 +762,9 @@
         w_value.T,
         w_mix_out,
         mix_taps,
-        cut(w_linear.T),
-        cut(w_gated.T),
-        cut(w_down),
+        w_linear.T,
+        w_gated.T,
+        w_down,
         ffn_taps,
         ffn_bias,
     )
@@ -688,7 +774,7 @@
     stream, w_value, w_linear = arrays[0], arrays[4], arrays[9]
     same = n_fs == n_tp == 2 * rep == 4
     whole = w_value.shape[0] % 128 == 0 and 2 * w_value.shape[1] % (CHUNKS * PACK) == 0
-    even = w_linear.shape[1] % (8 * n_fs) == 0 and stream.shape[0] == 2 * SEQ_LEN
+    even = w_linear.shape[1] % (2 * PACK) == 0 and stream.shape[0] == 2 * SEQ_LEN
     if same and whole and even:
         return split_plan(n_fs, *arrays)
     return gather_plan(*arrays)

time: 102 us -> 92.1 us (0.903)
  Pallas kernels: 99.6 us -> 91 us
  local copies, waits for them, and re-layouts: 2.06 us -> 0.88 us
    pallas_call x1, Pallas kernels: 99.6 us -> 91 us  [split_plan(): pl.pallas_call(functools.partial(kernel, n_fs, conv_w, tuple(spans)), out...]
    unnamed x1, local copies, waits for them, and re-layouts: 2.06 us -> 0.88 us
where the time goes in v3:
time: 92.1 us; the launch traced here: 91.9 us
  Pallas kernels  91 us (99%)
    pallas_call x1, Pallas kernels, split_plan(): pl.pallas_call(functools.partial(kernel, n_fs, conv_w, tuple(spans)), out...  91 us

profile of v3, /device:TPU:0, one launch (start us, length us, event | category | flops | bytes accessed | tf_op | source)
XLA Modules:
  0.0 91.9 jit_solution(4926144756825834128)
XLA Ops:
  0.0 91.0 %shard_map.145 = bf16[256,1536]{1,0:T(8,128)(2,1)S(1)} custom-call(bf16[256,1536]{1,0:T(8,128)(2,1)} %refs_0_.1, f32[1536]{0:T(1024)} %refs_1_.1, f32[1536]{0:T(1024)} %refs_2_.1, f32[1536]{0:T(1024)} %refs_3_.1, f32[1536]{0:T(1024)} %refs_4_.1, bf16[192,384]{1,0:T(8,128)(2,1)} %bitcast.7, bf16[192,384]{1,0:T(8,128)(2,1)} %bitcast.8, ...), custom_call_target="tpu_custom_call" | custom-call | tf_op jit(solution)/shard_map/pallas_call | solution.py:687
  91.0 0.9 copy.17

commit v4 on v3

--- a/solution.py
+++ b/solution.py
@@ -14,6 +14,7 @@
 SPREAD = 2
 PARTS = 4
 JOIN = 2
+FIRST = (0, 1)
 EDGE = (
     (),
     (),
@@ -22,10 +23,11 @@
 )
 INNER = (
     ((1, 0), (1, 1), (1, 2)),
-    (),
-    ((3, 0), (3, 1), (3, 2)),
-    ((2, 0), (2, 1), (2, 2)),
+    ((3, 0), (3, 1)),
+    ((3, 2), (2, 0), (2, 1)),
+    ((2, 2),),
 )
+SIDEWAYS = ((True, False, False, True), (True, True, True, False))
 TRACE = False
 
 
@@ -179,11 +181,10 @@
         az_r,
         ap_s,
         ap_r,
+        ac_r,
         rs_s,
         rs_r,
-        rp_s,
         rp_r,
-        rz_s,
         rz_r,
         rq_r,
         fin_s,
@@ -209,8 +210,6 @@
     upward, downward = mirror(jnp.where(inner, 2, 1)), mirror(0)
     places = [f] + order
 
-    started = []
-
     def send(src, dst, ss, rs, where):
         return pltpu.make_async_remote_copy(
             src_ref=src,
@@ -221,21 +220,26 @@
             device_id_type=pl.DeviceIdType.MESH,
         )
 
-    def start(copy, when=None):
-        started.append((copy, when))
+    owed = []
+
+    def owe(ref, sem, when=None):
+        owed.append((send(ref, ref, sem, sem, core), when))
+
+    def settle_sends():
+        for copy, when in owed:
+            if when is None:
+                copy.wait_send()
+            else:
+                pl.when(when)(copy.wait_send)
+
+    def begin(copy, when=None):
         if when is None:
             copy.start()
         else:
             pl.when(when)(copy.start)
 
-    def flush(count=None):
-        with scope("sends"):
-            for copy, when in started[:count]:
-                if when is None:
-                    copy.wait_send()
-                else:
-                    pl.when(when)(copy.wait_send)
-        del started[:count]
+    def landed(ref, sem, name):
+        wait(send(ref, ref, sem, sem, core), name)
 
     def wait(copy, name):
         with scope(name):
@@ -249,25 +253,29 @@
     targets += [stream, gain_mix_pre, w_linear, w_gated, w_down, ffn_taps, ffn_bias]
     targets += [gain_mix_post, gain_ffn_pre, gain_ffn_post, mix_taps]
     places_in = (5, 6, 7, 8, 0, 1, 10, 11, 12, 13, 14, 2, 3, 4, 9)
-    loads = [pltpu.make_async_copy(sources[i], ref, load_s.at[i]) for i, ref in zip(places_in, targets)]
+    loads = [
+        pltpu.make_async_copy(sources[i], ref, load_s.at[max(k - 3, 0)])
+        for k, (i, ref) in enumerate(zip(places_in, targets))
+    ]
     for load in loads:
         load.start()
-    for load in loads[:4]:
-        load.wait()
+    pltpu.make_async_copy(mix_all.at[f], mix_all.at[f], load_s.at[0]).wait()
     with scope("barrier"):
         pl.semaphore_wait(barrier, len(peers))
 
     mix_half = mix_all.shape[1] // 2
     mix_cut = mix_half // CHUNKS
 
-    def mix_copy(b, h, slot, to):
+    def mix_copy(b, h, to):
         at = pl.ds(pl.multiple_of(r * mix_half + h * mix_cut, PACK), mix_cut)
         ref = mix_all.at[b, at]
-        return send(ref, ref, mz_s.at[slot], mz_r.at[b, h], {"fs": to})
+        return send(ref, ref, mz_s.at[0], mz_r.at[b, h], {"fs": to})
 
     for h in range(CHUNKS):
-        start(mix_copy(f, h, h, upward))
-        start(mix_copy(f, h, CHUNKS + h, downward), inner)
+        begin(mix_copy(f, h, upward))
+        begin(mix_copy(f, h, downward), inner)
+    owe(mix_all.at[0, 0:mix_half], mz_s.at[0], edge)
+    owe(mix_all.at[0:n_fs, 0 : mix_half * 5 // n_fs], mz_s.at[0], inner)
 
     for load in loads[6:]:
         load.wait()
@@ -293,12 +301,13 @@
         for p in range(3):
             at = slice(0, narrow[kind][i])
             src, dst = ffn_w.at[goals[i], p, at], ffn_all.at[f, 0, p, at]
-            yield send(src, dst, fz_s.at[i, p], fz_r.at[f, p], {"fs": goals[i]})
+            yield send(src, dst, fz_s.at[i], fz_r.at[f, p], {"fs": goals[i]})
 
     kinds = (edge, inner)
     ffn_out = [[list(ffn_send(kind, i)) for i in range(3)] for kind in range(2)]
     for kind in range(2):
-        started.extend((copy, kinds[kind]) for copies in ffn_out[kind] for copy in copies)
+        for i in range(3):
+            owe(ffn_w.at[0, :, 0 : narrow[kind][i]], fz_s.at[i], kinds[kind])
 
     def ffn_start(kind, *which):
         for i in which:
@@ -307,9 +316,9 @@
 
     pl.when(edge)(functools.partial(ffn_start, 0, 0, 1, 2))
 
-    own_side = [send(ffn_w.at[f, p], ffn_all.at[f, 2, p], fx_s.at[0, p], fx_r.at[0, p], side) for p in range(3)]
-    for copy in own_side:
-        start(copy)
+    own_side = send(ffn_w.at[f], ffn_all.at[f, 2], fx_s.at[0], fx_r.at[0], side)
+    own_side.start()
+    owe(ffn_w.at[f], fx_s.at[0])
     for p in range(3):
         ffn_all[f, 0, p] = ffn_w[f, p]
     for j, (at, *both) in enumerate(spans):
@@ -333,8 +342,9 @@
             small_all[j, half, 3:4, 0:size] = ffn_bias[at : at + size][None]
     smalls[0] = small_all[f, r]
     smalls[1] = small_all[f, 1 - r]
-    small_copy = send(smalls.at[0], smalls.at[2], fx_s.at[4, 0], fx_r.at[4, 0], side)
-    start(small_copy)
+    small_copy = send(smalls.at[0], smalls.at[2], fx_s.at[1], fx_r.at[1], side)
+    small_copy.start()
+    owe(smalls.at[0], fx_s.at[1])
 
     for load in loads[4:6]:
         load.wait()
@@ -362,33 +372,35 @@
         b = jnp.where(inner, order[i_inner], order[i_edge])
         h = jnp.where(inner, h_inner, h_edge)
         onward = downward if i_inner > 0 else upward
-        copy = mix_copy(b, h, 2 * CHUNKS + e, onward)
+        copy = mix_copy(b, h, onward)
         wait(copy, f"mixz_{e}")
-        start(copy, inner)
+        begin(copy, inner)
         at = pl.ds(pl.multiple_of(r * mix_half + h * mix_cut, PACK), mix_cut)
         ref = mix_all.at[b, at]
-        my.append(send(ref, ref, my_s.at[e], my_r.at[e], other))
-        start(my[e])
+        my.append(send(ref, ref, my_s.at[0], my_r.at[e], other))
+        my[e].start()
         if e == 2 * CHUNKS - 2:
-            pl.when(inner)(functools.partial(ffn_start, 1, 0, 1))
+            pl.when(inner)(functools.partial(ffn_start, 1, *FIRST))
+    owe(mix_all.at[0:3, 0:mix_half], my_s.at[0])
     pl.when(inner)(functools.partial(ffn_start, 1, 2))
 
     def hop(kind, i, p, piece, ss, rs, to):
         src = ffn_all.at[places[i], 0, p, 0 : sizes[kind]]
         dst = ffn_all.at[places[i], piece, p, 0 : sizes[kind]]
-        return send(src, dst, ss.at[i, p], rs.at[i, p], to)
+        return send(src, dst, ss, rs, to)
 
     trips = [(i, p) for i in range(1, 4) for p in range(3)]
-    fy = [{(i, p): hop(kind, i, p, 1, fy_s, fy_r, other) for i, p in trips} for kind in range(2)]
-    fx = [{(i, p): hop(kind, i, p, 2, fx_s, fx_r, side) for i, p in trips} for kind in range(2)]
+    fy = [{(i, p): hop(kind, i, p, 1, fy_s.at[0], fy_r.at[0], other) for i, p in trips} for kind in range(2)]
+    fx = [{(i, p): hop(kind, i, p, 2, fx_s.at[2], fx_r.at[2], side) for i, p in trips} for kind in range(2)]
+    all_trips = [ffn_all.at[0:3, 0, :, 0 : sizes[kind]] for kind in range(2)]
     for kind in range(2):
-        for group in (fy, fx):
-            started.extend((copy, kinds[kind]) for copy in group[kind].values())
+        owe(all_trips[kind], fy_s.at[0], kinds[kind])
+        owe(all_trips[kind], fx_s.at[2], kinds[kind])
 
     def forward(kind, *which):
         for i, p in which:
             src = ffn_all.at[places[i], 0, p, 0 : sizes[kind]]
-            wait(send(src, src, fz_s.at[i - 1, p], fz_r.at[places[i], p], other), f"ffnz_{i}_{p}")
+            wait(send(src, src, fz_s.at[i - 1], fz_r.at[places[i], p], other), f"ffnz_{i}_{p}")
             fy[kind][i, p].start()
             fx[kind][i, p].start()
 
@@ -398,13 +410,12 @@
                 pl.when(kinds[kind])(functools.partial(forward, kind, *which))
 
     def arrived(kind):
-        for i, p in trips:
-            wait(fy[kind][i, p], f"ffny_{i}_{p}")
-            wait(fx[kind][i, p], f"ffnx_{i}_{p}")
+        landed(all_trips[kind], fy_r.at[0], "ffny")
+        landed(all_trips[kind], fx_r.at[2], "ffnx")
 
     relay(EDGE[0], INNER[0])
     for e in range(3 * CHUNKS):
-        if e == 3 * CHUNKS - 1:
+        if e == 2 * CHUNKS:
             relay(EDGE[1], INNER[1])
         wait(my[e], f"mixy_{e}")
         if e == 2 * CHUNKS - 1:
@@ -421,16 +432,17 @@
             pm[k, :, j * width : (j + 1) * width] = dot_nn(
                 mixed, mix_all[j, 3 * conv_w : 4 * conv_w]
             ).astype(jnp.bfloat16)
-        mix_core.append(send(pm.at[k, theirs], rm.at[k], mr_s.at[k], mr_r.at[k], core))
-        start(mix_core[k])
+        mix_core.append(send(pm.at[k, theirs], rm.at[k], mr_s.at[0], mr_r.at[k], core))
+        mix_core[k].start()
 
     def mix_sum(k):
         wait(mix_core[k], f"mixcore_{k}")
         return (pm[k, mine].astype(jnp.float32) + rm[k].astype(jnp.float32)).astype(jnp.bfloat16)
 
     sm[...] = mix_sum(0)
-    mix_side = send(sm, rxm, mr_s.at[2], mr_r.at[2], side)
-    start(mix_side)
+    mix_side = send(sm, rxm, mr_s.at[0], mr_r.at[2], side)
+    mix_side.start()
+    owe(rz.at[0:3], mr_s.at[0])
 
     kept = mix_sum(1)
     relay(EDGE[2], INNER[2])
@@ -442,7 +454,7 @@
     middle[...] = mid
     xs[f, 0, mine] = norm_rows(mid.astype(jnp.float32), gain_ffn_pre[...][None]).astype(jnp.bfloat16)
 
-    sideways = [edge == (i % 2 == 1) for i in range(4)]
+    sideways = [jnp.where(edge, a, b) for a, b in zip(*SIDEWAYS)]
     partner = [{"rep": jnp.where(a, r, 1 - r), "tp": jnp.where(a, t_side, t)} for a in sideways]
     cut = share // SPREAD
 
@@ -451,38 +463,35 @@
 
     ag_core, ag_pair, ag_pass = {}, {}, {}
 
-    def line_copy(i, a):
-        src = piece_of(places[i], 0, a)
-        onward = downward if i > 1 else upward
-        return send(src, src, az_s.at[1 + i, a], az_r.at[places[i], a], {"fs": onward})
-
-    ag_line = {(i, a): line_copy(i, a) for i in range(1, 4) for a in range(SPREAD)}
+    slab = pl.ds(pl.multiple_of(c * share, share), share)
+    slab_core = pl.ds(pl.multiple_of((1 - c) * share, share), share)
     for i in range(4):
         for a in range(SPREAD):
-            src = piece_of(places[i], 0, a)
-            ag_pair[i, a] = send(src, piece_of(places[i], 1, a), ap_s.at[0, i, a], ap_r.at[0, i, a], partner[i])
-            ag_core[i, a] = send(src, src, ap_s.at[1, i, a], ap_r.at[1, i, a], core)
-            started.extend(((ag_pair[i, a], None), (ag_core[i, a], None)))
-            if i > 0:
-                started.append((ag_line[i, a], inner))
-
-    def spread(i):
+            src, far = piece_of(places[i], 0, a), piece_of(places[i], 1, a)
+            ag_pair[i, a] = send(src, far, ap_s.at[0], ap_r.at[i, a], partner[i])
+            ag_core[i, a] = send(src, src, ap_s.at[1], ac_r.at[0, i], core)
+            ag_pass[i, a] = send(far, far, ap_s.at[2], ac_r.at[1, i], core)
+    for k in range(3):
+        owe(rz, ap_s.at[k])
+    owe(rz.at[0], az_s.at[0])
+    owe(rz, az_s.at[1], inner)
+
+    def pair_own():
         for a in range(SPREAD):
+            ag_pair[0, a].start()
+
+    def spread(i, which=range(SPREAD)):
+        for a in which:
             src = piece_of(places[i], 0, a)
             if i == 0:
-                start(send(src, src, az_s.at[0, a], az_r.at[places[i], a], {"fs": upward}))
-                start(send(src, src, az_s.at[1, a], az_r.at[places[i], a], {"fs": downward}), inner)
+                send(src, src, az_s.at[0], az_r.at[f, a], {"fs": upward}).start()
+                begin(send(src, src, az_s.at[1], az_r.at[f, a], {"fs": downward}), inner)
             else:
-                wait(ag_line[i, a], f"agz_{i}_{a}")
-                pl.when(inner)(ag_line[i, a].start)
-            ag_pair[i, a].start()
+                copy = send(src, src, az_s.at[1], az_r.at[places[i], a], {"fs": downward if i > 1 else upward})
+                wait(copy, f"agz_{i}_{a}")
+                begin(copy, inner)
+                ag_pair[i, a].start()
             ag_core[i, a].start()
-
-    for i in range(4):
-        for a in range(SPREAD):
-            src = piece_of(places[i], 1, a)
-            ag_pass[i, a] = send(src, src, ap_s.at[2, i, a], ap_r.at[2, i, a], core)
-            started.append((ag_pass[i, a], None))
 
     def pass_on(i):
         for a in range(SPREAD):
@@ -494,8 +503,7 @@
 
     def block(i):
         for s in range(2):
-            for a in range(SPREAD):
-                wait((ag_pass if s else ag_core)[i, a], f"agcore_{i}_{s}_{a}")
+            landed(xs.at[places[i], s, slab_core], ac_r.at[s, i], f"agcore_{i}_{s}")
         z = places[i]
         second = jnp.where(sideways[i], 1, 2)
         with scope(f"block_{i}"):
@@ -517,8 +525,8 @@
                 total = total.astype(jnp.bfloat16).reshape(2, SEQ_LEN, width)
                 pf[i, :, :, j * width : (j + 1) * width] = total
         for s in (1, 0):
-            rs_core[i, s] = send(pf.at[i, s, theirs], rf.at[i, s], rs_s.at[0, i, s], rs_r.at[0, i, s], core)
-            start(rs_core[i, s])
+            rs_core[i, s] = send(pf.at[i, s, theirs], rf.at[i, s], rs_s.at[0], rs_r.at[i, s], core)
+            rs_core[i, s].start()
 
     def stage_core(i, s):
         wait(rs_core[i, s], f"rscore_{i}_{s}")
@@ -528,23 +536,24 @@
             total = pf[i, s, ours].astype(jnp.float32) + rf[i, s, at].astype(jnp.float32)
             sf[i, s, at] = total.astype(jnp.bfloat16)
             if s:
-                rs_pair[i, a] = send(sf.at[i, s, at], rx.at[i, at], rp_s.at[i, a], rp_r.at[i, a], partner[i])
-                start(rs_pair[i, a])
-
-    rs_line, late = {}, []
+                rs_pair[i, a] = send(sf.at[i, s, at], rx.at[i, at], rs_s.at[1], rp_r.at[i, a], partner[i])
+                rs_pair[i, a].start()
+
+    rs_line = {}
     for i in range(1, 4):
         for a in range(PARTS):
             at = pl.ds(a * part, part)
-            home = send(tf.at[i, at], rz.at[f, at], rz_s.at[i, a], rz_r.at[f, a], {"fs": places[i]})
-            late.append((home, None if i == 1 else inner))
-            rs_line[i, a] = home, None
+            home = send(tf.at[i, at], rz.at[f, at], rs_s.at[2], rz_r.at[f, a], {"fs": places[i]})
+            near_by = None
             if i > 1:
-                near_by = send(tf.at[i, at], rq.at[i, at], rz_s.at[i, a], rq_r.at[i, a], {"fs": places[1]})
-                late.append((near_by, edge))
-                rs_line[i, a] = home, near_by
-
-    def stage_pair(i):
-        for a in range(PARTS):
+                near_by = send(tf.at[i, at], rq.at[i, at], rs_s.at[2], rq_r.at[i - 2, a], {"fs": places[1]})
+            rs_line[i, a] = home, near_by
+    owe(xs.at[:, 0], rs_s.at[0])
+    owe(rz, rs_s.at[1])
+    owe(rz.at[0:3], rs_s.at[2])
+
+    def stage_pair(i, which=range(PARTS)):
+        for a in which:
             at = pl.ds(a * part, part)
             wait(rs_pair[i, a], f"rspair_{i}_{a}")
             total = sf[i, 0, at].astype(jnp.float32) + rx[i, at].astype(jnp.float32)
@@ -572,55 +581,50 @@
         stage_core(i, 1)
         stage_core(i, 0)
 
+    half = SPREAD // 2
     spread(0)
     relay(EDGE[3], INNER[3])
 
     @pl.when(edge)
     def _():
-        pass_on(0)
         spread(1)
+        pair_own()
         spread(2)
+        pass_on(1)
         arrived(0)
+        spread(3, range(half))
 
     @pl.when(inner)
     def _():
         spread(1)
         spread(2)
         spread(3)
-        pass_on(0)
+        pair_own()
+        pass_on(1)
         arrived(1)
 
-    for copy in own_side + [small_copy]:
-        wait(copy, "ffnown")
+    wait(own_side, "ffnown")
+    wait(small_copy, "small")
+    block(1)
+    pl.when(edge)(functools.partial(spread, 3, range(half, SPREAD)))
+    pass_on(2)
+    stage(1)
+    block(2)
+    pass_on(3)
+    stage_pair(1, (0,))
+    stage(2)
+    stage_pair(1, (1,))
+    block(3)
+    stage_pair(1, range(2, PARTS))
+    pass_on(0)
+    stage(3)
+    pl.when(edge)(functools.partial(stage_pair, 2, (0, 1)))
     block(0)
-    pass_on(1)
-    pl.when(edge)(functools.partial(spread, 3))
-    pass_on(2)
-    early = len(started)
-    block(1)
-    block(2)
-    stage(1)
-    pass_on(3)
-    stage(2)
+    pl.when(edge)(functools.partial(stage_pair, 2, range(2, PARTS)))
     stage(0)
-    block(3)
-    stage(3)
-
-    @pl.when(edge)
-    def _():
-        stage_pair(2)
-        stage_pair(3)
-        stage_pair(1)
-
-    @pl.when(inner)
-    def _():
-        stage_pair(1)
-        stage_pair(2)
-        stage_pair(3)
-
+    pl.when(inner)(functools.partial(stage_pair, 2))
+    stage_pair(3)
     stage_pair(0)
-    flush(early)
-    started.extend(late)
 
     def row_slot(who, a):
         return pl.ds(pl.multiple_of(who * share + a * part, part), part)
@@ -631,25 +635,23 @@
         total = tf[0, at].astype(jnp.float32)
         for i in range(1, 3):
             ref = rz.at[places[i], at]
-            wait(send(ref, ref, rz_s.at[0, a], rz_r.at[places[i], a], {"fs": places[i]}), f"rz_{i}_{a}")
+            landed(ref, rz_r.at[places[i], a], f"rz_{i}_{a}")
             total = total + rz[places[i], at].astype(jnp.float32)
         branch = total.astype(jnp.bfloat16).astype(jnp.float32)
         done = middle[at].astype(jnp.float32) + norm_rows(branch, gain_ffn_post[...][None])
         out[row_slot(t, a)] = done.astype(jnp.bfloat16)
         own = out.at[row_slot(t, a)]
-        for k, to in enumerate((side, core)):
-            fin[k, a] = send(own, own, fin_s.at[k, a], fin_r.at[k, a], to)
-            start(fin[k, a])
+        fin[a] = send(own, own, fin_s.at[0], fin_r.at[a], side)
+        fin[a].start()
+        send(own, own, fin_s.at[0], fin_r.at[PARTS], core).start()
     for a in range(PARTS):
-        wait(fin[0, a], f"finside_{a}")
+        wait(fin[a], f"finside_{a}")
         far = out.at[row_slot(t_side, a)]
-        fin[2, a] = send(far, far, fin_s.at[2, a], fin_r.at[2, a], core)
-        start(fin[2, a])
-    for a in range(PARTS):
-        wait(fin[1, a], f"fincore_{a}")
-        wait(fin[2, a], f"finpass_{a}")
-
-    flush()
+        send(far, far, fin_s.at[0], fin_r.at[PARTS + 1], core).start()
+    for k in range(2):
+        landed(rz.at[0], fin_r.at[PARTS + k], f"fincore_{k}")
+    owe(rz.at[0:3], fin_s.at[0])
+    settle_sends()
 
 
 def split_plan(
@@ -701,7 +703,7 @@
             vmem(w_down.shape, half),
             vmem(ffn_taps.shape, jnp.float32),
             vmem(ffn_bias.shape, jnp.float32),
-            dma((15,)),
+            dma((12,)),
             vmem((n_fs, 2, 8, cap), jnp.float32),
             vmem((3, 8, cap), jnp.float32),
             vmem((n_fs, 3, cap, width), half),
@@ -722,31 +724,30 @@
             vmem((n_fs, share, model), half),
             vmem((n_fs, share, model), half),
             vmem((n_fs, share, model), half),
-            dma((5 * CHUNKS,)),
+            dma((1,)),
             dma((n_fs, CHUNKS)),
+            dma((1,)),
             dma((3 * CHUNKS,)),
-            dma((3 * CHUNKS,)),
+            dma((1,)),
             dma((3,)),
             dma((3,)),
-            dma((3, 3)),
             dma((n_fs, 3)),
-            dma((n_fs, 3)),
-            dma((n_fs, 3)),
-            dma((5, 3)),
-            dma((5, 3)),
-            dma((5, SPREAD)),
+            dma((1,)),
+            dma((1,)),
+            dma((3,)),
+            dma((3,)),
+            dma((2,)),
             dma((n_fs, SPREAD)),
-            dma((3, n_fs, SPREAD)),
-            dma((3, n_fs, SPREAD)),
-            dma((1, n_fs, 2)),
-            dma((1, n_fs, 2)),
+            dma((3,)),
+            dma((n_fs, SPREAD)),
+            dma((2, n_fs)),
+            dma((3,)),
+            dma((n_fs, 2)),
             dma((n_fs, PARTS)),
             dma((n_fs, PARTS)),
-            dma((n_fs, PARTS)),
-            dma((n_fs, PARTS)),
-            dma((n_fs, PARTS)),
-            dma((3, PARTS)),
-            dma((3, PARTS)),
+            dma((2, PARTS)),
+            dma((1,)),
+            dma((PARTS + 2,)),
         ],
         compiler_params=pltpu.CompilerParams(
             collective_id=0, has_side_effects=True, vmem_limit_bytes=58 * 2**20

time: 92.1 us -> 89.8 us (0.975)
  Pallas kernels: 91 us -> 88.8 us
    pallas_call x1, Pallas kernels: 91 us -> 88.8 us  [split_plan(): pl.pallas_call(functools.partial(kernel, n_fs, conv_w, tuple(spans)), out...]
where the time goes in v4:
time: 89.8 us; the launch traced here: 89.7 us
  Pallas kernels  88.8 us (99%)
    pallas_call x1, Pallas kernels, split_plan(): pl.pallas_call(functools.partial(kernel, n_fs, conv_w, tuple(spans)), out...  88.8 us

profile of v4, /device:TPU:0, one launch (start us, length us, event | category | flops | bytes accessed | tf_op | source)
XLA Modules:
  0.0 89.7 jit_solution(14289472494192210381)
XLA Ops:
  0.0 88.8 %shard_map.145 = bf16[256,1536]{1,0:T(8,128)(2,1)S(1)} custom-call(bf16[256,1536]{1,0:T(8,128)(2,1)} %refs_0_.1, f32[1536]{0:T(1024)} %refs_1_.1, f32[1536]{0:T(1024)} %refs_2_.1, f32[1536]{0:T(1024)} %refs_3_.1, f32[1536]{0:T(1024)} %refs_4_.1, bf16[192,384]{1,0:T(8,128)(2,1)} %bitcast.7, bf16[192,384]{1,0:T(8,128)(2,1)} %bitcast.8, ...), custom_call_target="tpu_custom_call" | custom-call | tf_op jit(solution)/shard_map/pallas_call | solution.py:689
  88.8 0.9 copy.17

commit v5 on v4

--- a/solution.py
+++ b/solution.py
@@ -147,6 +147,7 @@
         load_s,
         small_all,
         smalls,
+        small_pair,
         ffn_w,
         ffn_all,
         mix_all,
@@ -501,29 +502,45 @@
     rs_core, rs_pair = {}, {}
     part = share // PARTS
 
+    def activate(linear, gated, small):
+        linear = linear.astype(jnp.bfloat16).astype(jnp.float32)
+        gated = gated.astype(jnp.bfloat16).astype(jnp.float32)
+        act = jax.nn.gelu(conv_rows(gated, small) + small[3:4], approximate=True)
+        return (act * linear).astype(jnp.bfloat16)
+
+    def raise_up(z, weights):
+        linear, gated = 0.0, 0.0
+        for j in range(0, n_fs, JOIN):
+            act = xs[z, :, :, j * width : (j + JOIN) * width].reshape(2 * SEQ_LEN, JOIN * width)
+            joined = lambda p: jnp.concatenate([weights(j + k, p) for k in range(JOIN)], axis=1)
+            linear = linear + dot_nt(act, joined(0))
+            gated = gated + dot_nt(act, joined(1))
+        return linear, gated
+
+    def keep_partial(i, j, total):
+        pf[i, :, :, j * width : (j + 1) * width] = total.astype(jnp.bfloat16).reshape(2, SEQ_LEN, width)
+
+    def block_edge(i):
+        second = 1 if SIDEWAYS[0][i] else 2
+        both = lambda j, p: jnp.concatenate([ffn_all[j, h, p, 0:few] for h in (0, second)], axis=0)
+        hidden = activate(*raise_up(places[i], both), small_pair[second - 1])
+        for j in range(n_fs):
+            keep_partial(i, j, dot_nn(hidden, both(j, 2)))
+
+    def block_inner(i):
+        second = 1 if SIDEWAYS[1][i] else 2
+        hidden = [
+            activate(*raise_up(places[i], lambda j, p: ffn_all[j, h, p]), smalls[h]) for h in (0, second)
+        ]
+        for j in range(n_fs):
+            total = dot_nn(hidden[0], ffn_all[j, 0, 2]) + dot_nn(hidden[1], ffn_all[j, second, 2])
+            keep_partial(i, j, total)
+
     def block(i):
         for s in range(2):
             landed(xs.at[places[i], s, slab_core], ac_r.at[s, i], f"agcore_{i}_{s}")
-        z = places[i]
-        second = jnp.where(sideways[i], 1, 2)
-        with scope(f"block_{i}"):
-            hidden = []
-            for h in (0, second):
-                linear, gated = 0.0, 0.0
-                for j in range(0, n_fs, JOIN):
-                    act = xs[z, :, :, j * width : (j + JOIN) * width].reshape(2 * SEQ_LEN, JOIN * width)
-                    joined = lambda p: jnp.concatenate([ffn_all[j + k, h, p] for k in range(JOIN)], axis=1)
-                    linear = linear + dot_nt(act, joined(0))
-                    gated = gated + dot_nt(act, joined(1))
-                linear = linear.astype(jnp.bfloat16).astype(jnp.float32)
-                gated = gated.astype(jnp.bfloat16).astype(jnp.float32)
-                small = smalls[h]
-                act = jax.nn.gelu(conv_rows(gated, small) + small[3:4], approximate=True)
-                hidden.append((act * linear).astype(jnp.bfloat16))
-            for j in range(n_fs):
-                total = dot_nn(hidden[0], ffn_all[j, 0, 2]) + dot_nn(hidden[1], ffn_all[j, second, 2])
-                total = total.astype(jnp.bfloat16).reshape(2, SEQ_LEN, width)
-                pf[i, :, :, j * width : (j + 1) * width] = total
+        for kind in range(2):
+            pl.when(kinds[kind])(functools.partial((block_edge, block_inner)[kind], i))
         for s in (1, 0):
             rs_core[i, s] = send(pf.at[i, s, theirs], rf.at[i, s], rs_s.at[0], rs_r.at[i, s], core)
             rs_core[i, s].start()
@@ -581,7 +598,6 @@
         stage_core(i, 1)
         stage_core(i, 0)
 
-    half = SPREAD // 2
     spread(0)
     relay(EDGE[3], INNER[3])
 
@@ -592,7 +608,6 @@
         spread(2)
         pass_on(1)
         arrived(0)
-        spread(3, range(half))
 
     @pl.when(inner)
     def _():
@@ -605,8 +620,11 @@
 
     wait(own_side, "ffnown")
     wait(small_copy, "small")
+    for k in range(2):
+        small_pair[k, :, 0:few] = smalls[0, :, 0:few]
+        small_pair[k, :, few : 2 * few] = smalls[k + 1, :, 0:few]
     block(1)
-    pl.when(edge)(functools.partial(spread, 3, range(half, SPREAD)))
+    pl.when(edge)(functools.partial(spread, 3))
     pass_on(2)
     stage(1)
     block(2)
@@ -706,6 +724,7 @@
             dma((12,)),
             vmem((n_fs, 2, 8, cap), jnp.float32),
             vmem((3, 8, cap), jnp.float32),
+            vmem((2, 8, 2 * few), jnp.float32),
             vmem((n_fs, 3, cap, width), half),
             vmem((n_fs, 3, 3, cap, width), half),
             vmem((n_fs, 4 * conv_w, width), half),

time: 89.8 us -> 88.9 us (0.990)
  Pallas kernels: 88.8 us -> 87.9 us
where the time goes in v5:
time: 88.9 us; the launch traced here: 88.8 us
  Pallas kernels  87.9 us (99%)
    pallas_call x1, Pallas kernels, split_plan(): pl.pallas_call(functools.partial(kernel, n_fs, conv_w, tuple(spans)), out...  87.9 us

profile of v5, /device:TPU:0, one launch (start us, length us, event | category | flops | bytes accessed | tf_op | source)
XLA Modules:
  0.0 88.8 jit_solution(12257503998727649115)
XLA Ops:
  0.0 87.9 %shard_map.145 = bf16[256,1536]{1,0:T(8,128)(2,1)S(1)} custom-call(bf16[256,1536]{1,0:T(8,128)(2,1)} %refs_0_.1, f32[1536]{0:T(1024)} %refs_1_.1, f32[1536]{0:T(1024)} %refs_2_.1, f32[1536]{0:T(1024)} %refs_3_.1, f32[1536]{0:T(1024)} %refs_4_.1, bf16[192,384]{1,0:T(8,128)(2,1)} %bitcast.7, bf16[192,384]{1,0:T(8,128)(2,1)} %bitcast.8, ...), custom_call_target="tpu_custom_call" | custom-call | tf_op jit(solution)/shard_map/pallas_call | solution.py:707
  87.9 0.9 copy.17

commit v6 on v5

--- a/solution.py
+++ b/solution.py
@@ -636,9 +636,9 @@
     stage_pair(1, range(2, PARTS))
     pass_on(0)
     stage(3)
-    pl.when(edge)(functools.partial(stage_pair, 2, (0, 1)))
+    pl.when(edge)(functools.partial(stage_pair, 2, (0,)))
     block(0)
-    pl.when(edge)(functools.partial(stage_pair, 2, range(2, PARTS)))
+    pl.when(edge)(functools.partial(stage_pair, 2, range(1, PARTS)))
     stage(0)
     pl.when(inner)(functools.partial(stage_pair, 2))
     stage_pair(3)

time: 88.9 us -> 89.2 us (level)
  no operation moved by 1% of the time
where the time goes in v6:
time: 89.2 us; the launch traced here: 89 us
  Pallas kernels  88.1 us (99%)
    pallas_call x1, Pallas kernels, split_plan(): pl.pallas_call(functools.partial(kernel, n_fs, conv_w, tuple(spans)), out...  88.1 us

profile of v6, /device:TPU:0, one launch (start us, length us, event | category | flops | bytes accessed | tf_op | source)
XLA Modules:
  0.0 89.0 jit_solution(2969446235948610720)
XLA Ops:
  0.0 88.1 %shard_map.145 = bf16[256,1536]{1,0:T(8,128)(2,1)S(1)} custom-call(bf16[256,1536]{1,0:T(8,128)(2,1)} %refs_0_.1, f32[1536]{0:T(1024)} %refs_1_.1, f32[1536]{0:T(1024)} %refs_2_.1, f32[1536]{0:T(1024)} %refs_3_.1, f32[1536]{0:T(1024)} %refs_4_.1, bf16[192,384]{1,0:T(8,128)(2,1)} %bitcast.7, bf16[192,384]{1,0:T(8,128)(2,1)} %bitcast.8, ...), custom_call_target="tpu_custom_call" | custom-call | tf_op jit(solution)/shard_map/pallas_call | solution.py:707
  88.1 0.9 copy.17
